TPU v7x, 32 devices: a whole 2x2x4 slice. The times are simulated.
32 devices in a mesh: ep: 4 (over y, x), tp: 8 (over z, core).
Axes of the slice: x: 2, y: 2, z: 4, core: 2. Of those that a mesh axis runs over, the one named last changes fastest.
Arguments:
- resid: bfloat16 [512, 2048], P('ep'), may hold values from -6 to 6
- norm1_gain: float32 [2048], replicated, may hold values from 0.1 to 1.9
- w_query: bfloat16 [2048, 2048], P('ep', 'tp'), may hold values from -0.125 to 0.125
- w_key: bfloat16 [2048, 2048], P('ep', 'tp'), may hold values from -0.125 to 0.125
- w_value: bfloat16 [2048, 2048], P('ep', 'tp'), may hold values from -0.125 to 0.125
- w_outgate: bfloat16 [2048, 2048], P('ep', 'tp'), may hold values from -0.125 to 0.125
- w_igate: bfloat16 [2048, 32], replicated, may hold values from -0.125 to 0.125
- w_fgate: bfloat16 [2048, 32], replicated, may hold values from -0.125 to 0.125
- forget_bias: float32 [32], replicated, may hold values from 0 to 4
- head_gain: float32 [2048], P('tp'), may hold values from 0.1 to 1.9
- w_out: bfloat16 [2048, 2048], P('tp'), may hold values from -0.125 to 0.125
- state_matrix: float32 [512, 32, 64, 64], P('ep', 'tp'), may hold values from -4 to 4
- state_norm: float32 [512, 32, 64], P('ep', 'tp'), may hold values from -8 to 8
- state_max: float32 [512, 32], P('ep', 'tp'), may hold values from -1 to 2
- norm2_gain: float32 [2048], replicated, may hold values from 0.1 to 1.9
- group_router: bfloat16 [2048, 4], replicated, may hold values from -0.125 to 0.125
- expert_router: bfloat16 [2048, 8], replicated, may hold values from -0.125 to 0.125
- expert_ids: int32 [512, 2], P('ep'), may hold values from 0 to 7, all different within a row; in each aligned block of 128 rows (0 to 127, 128 to 255, ...) at most 48 rows name the same one
- exp_gate: bfloat16 [8, 2048, 1024], P('ep', None, 'tp'), may hold values from -0.125 to 0.125
- exp_up: bfloat16 [8, 2048, 1024], P('ep', None, 'tp'), may hold values from -0.125 to 0.125
- exp_down: bfloat16 [8, 1024, 2048], P('ep', 'tp'), may hold values from -0.1875 to 0.1875
Outputs:
- mixed: bfloat16 [512, 2048], P('ep', 'tp')
- new_matrix: float32 [512, 32, 64, 64], P('ep', 'tp')
- new_normer: float32 [512, 32, 64], P('ep', 'tp')
- new_max: float32 [512, 32], P('ep', 'tp')
Inputs may be any that keep to these rules, and one draw needn't show every extreme that they name: `expert_ids`: A token's 2 experts differ. Among the 128 tokens of one index of ep (aligned blocks of rows) no expert is named more than 48 times, and in some block one expert is named exactly 48 times.
All inputs are finite; a program needn't handle non-finite values.
Results may differ from a plain program's by a relative error of at most 0.014.
Values may be sent and summed in bfloat16 or wider, within the bound.
A program may use at most 128 MiB of HBM per device.

v0:
```python
import functools

import jax
import jax.numpy as jnp
from jax import lax
from jax.experimental import pallas as pl
from jax.experimental.pallas import tpu as pltpu
from jax.sharding import PartitionSpec as P

EPSILON = 1e-06


def rms_scale(values, gain):
    widened = values.astype(jnp.float32)
    factor = lax.rsqrt(jnp.mean(widened * widened, axis=-1, keepdims=True) + EPSILON)
    return widened * factor * gain


def memory_cell(scaled, key_rows, value_rows, in_gate, log_forget, matrix, normer, running):
    stable = jnp.maximum(log_forget + running, in_gate)
    fresh = jnp.exp(in_gate - stable)
    carried = jnp.exp(log_forget + running - stable)
    readout = jnp.einsum("bhd,bhde->bhe", scaled, matrix, precision=lax.Precision.HIGHEST)
    score = jnp.sum(scaled * key_rows, axis=-1) * fresh
    numer = carried[..., None] * readout + score[..., None] * value_rows
    denom = carried * jnp.sum(scaled * normer, axis=-1) + score
    cell_out = numer / jnp.maximum(jnp.abs(denom), 1.0)[..., None]
    new_matrix = (
        carried[..., None, None] * matrix
        + fresh[..., None, None] * key_rows[..., :, None] * value_rows[..., None, :]
    )
    new_normer = carried[..., None] * normer + fresh[..., None] * key_rows
    return (cell_out, new_matrix, new_normer, stable)


MESH = pl.DeviceIdType.MESH
VMEM = pl.BlockSpec(memory_space=pltpu.VMEM)
ANY = pl.BlockSpec(memory_space=pl.ANY)


def remote(src, dst, send_sem, recv_sem, device):
    return pltpu.make_async_remote_copy(
        src_ref=src,
        dst_ref=dst,
        send_sem=send_sem,
        recv_sem=recv_sem,
        device_id=device,
        device_id_type=MESH,
    )


def greet(devices):
    barrier = pltpu.get_barrier_semaphore()
    for device in devices:
        pl.semaphore_signal(barrier, inc=1, device_id=device, device_id_type=MESH)


def project_kernel(
    n, resid, gain, wq, wk, wv, wo, wi, wf, out, in_gate, forget,
    blocks, arrived, sent, returned, weights, total, wsem, fs, fr, rs, rr,
):
    me = lax.axis_index("ep")
    ahead = [lax.rem(me + k, n) for k in range(n)]
    behind = [lax.rem(me + n - k, n) for k in range(n)]
    greet([{"ep": ahead[k]} for k in range(1, n)])
    width = wq.shape[1]
    depth = wq.shape[0]
    loads = []
    for i, w in enumerate((wq, wk, wv, wo)):
        load = pltpu.make_async_copy(w, weights.at[:, i * width : (i + 1) * width], wsem.at[i])
        load.start()
        loads.append(load)
    normed = rms_scale(resid[...], gain[...]).astype(jnp.bfloat16)
    for j in range(n):
        blocks[j] = normed[:, j * depth : (j + 1) * depth]
    pl.semaphore_wait(pltpu.get_barrier_semaphore(), n - 1)
    forward = {}
    for k in range(1, n):
        forward[k] = remote(blocks.at[ahead[k]], arrived.at[k], fs.at[k], fr.at[k], {"ep": ahead[k]})
        forward[k].start()
    in_gate[...] = jnp.dot(normed, wi[...], preferred_element_type=jnp.float32)
    forget[...] = jnp.dot(normed, wf[...], preferred_element_type=jnp.float32)
    for load in loads:
        load.wait()
    total[...] = jnp.dot(blocks[me], weights[...], preferred_element_type=jnp.float32)
    back = {}
    for k in range(1, n):
        forward[k].wait_recv()
        sent[k] = jnp.dot(arrived[k], weights[...], preferred_element_type=jnp.float32).astype(
            jnp.bfloat16
        )
        back[k] = remote(sent.at[k], returned.at[k], rs.at[k], rr.at[k], {"ep": behind[k]})
        back[k].start()
    for k in range(1, n):
        back[k].wait_recv()
        total[...] += returned[k].astype(jnp.float32)
    out[...] = total[...].astype(jnp.bfloat16)
    for k in range(1, n):
        forward[k].wait_send()
        back[k].wait_send()


def project(resid, gain, wq, wk, wv, wo, wi, wf):
    n = lax.axis_size("ep")
    rows = resid.shape[0]
    depth, width = wq.shape
    dma = pltpu.SemaphoreType.DMA
    bf16, f32 = jnp.bfloat16, jnp.float32
    return pl.pallas_call(
        functools.partial(project_kernel, n),
        out_shape=(
            jax.ShapeDtypeStruct((rows, 4 * width), bf16),
            jax.ShapeDtypeStruct((rows, wi.shape[1]), f32),
            jax.ShapeDtypeStruct((rows, wi.shape[1]), f32),
        ),
        in_specs=[VMEM, VMEM, ANY, ANY, ANY, ANY, VMEM, VMEM],
        out_specs=(VMEM, VMEM, VMEM),
        scratch_shapes=[
            pltpu.VMEM((n, rows, depth), bf16),
            pltpu.VMEM((n, rows, depth), bf16),
            pltpu.VMEM((n, rows, 4 * width), bf16),
            pltpu.VMEM((n, rows, 4 * width), bf16),
            pltpu.VMEM((depth, 4 * width), bf16),
            pltpu.VMEM((rows, 4 * width), f32),
            dma((4,)), dma((n,)), dma((n,)), dma((n,)), dma((n,)),
        ],
        compiler_params=pltpu.CompilerParams(
            collective_id=0, has_side_effects=True, vmem_limit_bytes=32 * 1024 * 1024
        ),
    )(resid, gain.reshape(1, -1), wq, wk, wv, wo, wi, wf)


def mix_kernel(
    nt, head, w, own_cols, after_out, full_out,
    full, pair_s, pair_r, red_s, red_r, gathered, ps, pr, rs, rr, gs, gr, os, orr,
):
    t = lax.axis_index("tp")
    nz = nt // 2
    z, c = t // 2, lax.rem(t, 2)
    partner = {"tp": t + 1 - 2 * c}
    ahead = [lax.rem(z + k, nz) for k in range(nz)]
    behind = [lax.rem(z + nz - k, nz) for k in range(nz)]
    peers = [{"tp": 2 * ahead[k] + c} for k in range(nz)]
    greet([partner] + peers[1:])
    cols = own_cols.shape[1]
    full[...] = jnp.dot(head[...], w[...], preferred_element_type=jnp.float32)

    def block(dest):
        return full[:, pl.ds(pl.multiple_of(dest * cols, cols), cols)]

    for k in range(nz):
        pair_s[k] = block(2 * ahead[k] + 1 - c).astype(jnp.bfloat16)
    pl.semaphore_wait(pltpu.get_barrier_semaphore(), nz)
    order = list(range(1, nz)) + [0]
    pair = {}
    for k in order:
        pair[k] = remote(pair_s.at[k], pair_r.at[k], ps.at[k], pr.at[k], partner)
        pair[k].start()
    reduce = {}
    for k in order:
        pair[k].wait_recv()
        value = block(2 * ahead[k] + c) + pair_r[k].astype(jnp.float32)
        if k == 0:
            total = value
        else:
            red_s[k] = value.astype(jnp.bfloat16)
            reduce[k] = remote(red_s.at[k], red_r.at[k], rs.at[k], rr.at[k], peers[k])
            reduce[k].start()
    for k in range(1, nz):
        reduce[k].wait_recv()
        total = total + red_r[k].astype(jnp.float32)
    after = (own_cols[...].astype(jnp.float32) + total).astype(jnp.bfloat16)
    after_out[...] = after
    gathered[t] = after
    gather, over = {}, {}
    for k in range(1, nz):
        gather[k] = remote(gathered.at[t], gathered.at[t], gs.at[k], gr.at[k], peers[k])
        gather[k].start()
    for k in range(nz):
        origin = 2 * behind[k] + c
        if k > 0:
            gather[k].wait_recv()
        over[k] = remote(gathered.at[origin], gathered.at[origin], os.at[k], orr.at[k], partner)
        over[k].start()
    for k in range(nz):
        over[k].wait_recv()
    for j in range(nt):
        full_out[:, j * cols : (j + 1) * cols] = gathered[j]
    for k in range(nz):
        pair[k].wait_send()
        over[k].wait_send()
        if k > 0:
            reduce[k].wait_send()
            gather[k].wait_send()


def mix(head, w, own_cols):
    nt = lax.axis_size("tp")
    nz = nt // 2
    rows, cols = own_cols.shape
    dma = pltpu.SemaphoreType.DMA
    bf16, f32 = jnp.bfloat16, jnp.float32
    return pl.pallas_call(
        functools.partial(mix_kernel, nt),
        out_shape=(
            jax.ShapeDtypeStruct((rows, cols), bf16),
            jax.ShapeDtypeStruct((rows, cols * nt), bf16),
        ),
        in_specs=[VMEM, VMEM, VMEM],
        out_specs=(VMEM, VMEM),
        scratch_shapes=[
            pltpu.VMEM((rows, cols * nt), f32),
            pltpu.VMEM((nz, rows, cols), bf16),
            pltpu.VMEM((nz, rows, cols), bf16),
            pltpu.VMEM((nz, rows, cols), bf16),
            pltpu.VMEM((nz, rows, cols), bf16),
            pltpu.VMEM((nt, rows, cols), bf16),
        ]
        + [dma((nz,))] * 8,
        compiler_params=pltpu.CompilerParams(
            collective_id=1, has_side_effects=True, vmem_limit_bytes=32 * 1024 * 1024
        ),
    )(head, w, own_cols)


def expert_kernel(
    n, nt, disp, comb, wg, wu, wd, out,
    arr, vg, vu, vd, full, pair_s, pair_r, ret_s, ret_r, z_s, z_r,
    wsem, ds, dr, fs, fr, ps, pr, rs, rr, zs, zr,
):
    me = lax.axis_index("ep")
    t = lax.axis_index("tp")
    nz = nt // 2
    z, c = t // 2, lax.rem(t, 2)
    partner = {"tp": t + 1 - 2 * c}
    ahead = [lax.rem(me + k, n) for k in range(n)]
    behind = [lax.rem(me + n - k, n) for k in range(n)]
    z_ahead = [lax.rem(z + k, nz) for k in range(nz)]
    z_peers = [{"tp": 2 * z_ahead[k] + c} for k in range(nz)]
    greet([{"ep": ahead[k]} for k in range(1, n)] + [partner] + z_peers[1:])
    loads = []
    for i, (w, v) in enumerate(((wg, vg), (wu, vu), (wd, vd))):
        load = pltpu.make_async_copy(w, v, wsem.at[i])
        load.start()
        loads.append(load)
    half = arr.shape[3]
    local = vg.shape[0]
    cap = disp.shape[1] // local
    cols = out.shape[1]
    pl.semaphore_wait(pltpu.get_barrier_semaphore(), n - 1 + nz)
    mine = pl.ds(pl.multiple_of(c * half, half), half)
    send, pass_on, pair, ret = {}, {}, {}, {}
    for k in range(1, n):
        send[k] = remote(
            disp.at[ahead[k], :, mine], arr.at[c, k], ds.at[k], dr.at[k], {"ep": ahead[k]}
        )
        send[k].start()
    arr[0, 0] = disp[me, :, :half]
    arr[1, 0] = disp[me, :, half:]
    for load in loads:
        load.wait()

    def block(k, dest):
        return full[k, :, pl.ds(pl.multiple_of(dest * cols, cols), cols)]

    def compute(k):
        for e in range(local):
            lines = slice(e * cap, (e + 1) * cap)
            low, high = arr[0, k, lines, :], arr[1, k, lines, :]

            def both(v):
                return jnp.dot(
                    low, v[e, :half, :], preferred_element_type=jnp.float32
                ) + jnp.dot(high, v[e, half:, :], preferred_element_type=jnp.float32)

            units = (jax.nn.silu(both(vg)) * both(vu)).astype(jnp.bfloat16)
            full[k, lines, :] = jnp.dot(units, vd[e], preferred_element_type=jnp.float32)
        for i in range(nz):
            pair_s[k, i] = block(k, 2 * i + 1 - c).astype(jnp.bfloat16)
        pair[k] = remote(pair_s.at[k], pair_r.at[k], ps.at[k], pr.at[k], partner)
        pair[k].start()

    def reply(k):
        pair[k].wait_recv()
        for i in range(nz):
            ret_s[k, i] = (block(k, 2 * i + c) + pair_r[k, i].astype(jnp.float32)).astype(
                jnp.bfloat16
            )
        if k > 0:
            ret[k] = remote(ret_s.at[k], ret_r.at[k], rs.at[k], rr.at[k], {"ep": behind[k]})
            ret[k].start()

    compute(0)
    for k in range(1, n):
        send[k].wait_recv()
        pass_on[k] = remote(arr.at[c, k], arr.at[c, k], fs.at[k], fr.at[k], partner)
        pass_on[k].start()
        pass_on[k].wait_recv()
        compute(k)
        reply(k)
    reply(0)
    ret_r[0] = ret_s[0]
    weights = []
    for k in range(n):
        exact = comb[ahead[k]]
        coarse = exact.astype(jnp.bfloat16)
        weights.append((coarse, (exact - coarse.astype(jnp.float32)).astype(jnp.bfloat16)))
        if k > 0:
            ret[k].wait_recv()
    gather = {}
    for i in list(range(1, nz)) + [0]:
        total = jnp.zeros(out.shape, jnp.float32)
        for k in range(n):
            part = ret_r[k, z_ahead[i]]
            for weight in weights[k]:
                total = total + jnp.dot(weight, part, preferred_element_type=jnp.float32)
        if i > 0:
            z_s[i] = total.astype(jnp.bfloat16)
            gather[i] = remote(z_s.at[i], z_r.at[i], zs.at[i], zr.at[i], z_peers[i])
            gather[i].start()
    for i in range(1, nz):
        gather[i].wait_recv()
        total = total + z_r[i].astype(jnp.float32)
    out[...] = total
    for k in range(n):
        pair[k].wait_send()
        if k > 0:
            send[k].wait_send()
            pass_on[k].wait_send()
            ret[k].wait_send()
    for i in range(1, nz):
        gather[i].wait_send()


def experts(disp, comb, wg, wu, wd):
    n, nt = lax.axis_size("ep"), lax.axis_size("tp")
    nz = nt // 2
    slots, width = disp.shape[1:]
    rows = comb.shape[1]
    cols = width // nt
    dma = pltpu.SemaphoreType.DMA
    bf16, f32 = jnp.bfloat16, jnp.float32
    return pl.pallas_call(
        functools.partial(expert_kernel, n, nt),
        out_shape=jax.ShapeDtypeStruct((rows, cols), f32),
        in_specs=[VMEM, VMEM, ANY, ANY, ANY],
        out_specs=VMEM,
        scratch_shapes=[
            pltpu.VMEM((2, n, slots, width // 2), bf16),
            pltpu.VMEM(wg.shape, bf16),
            pltpu.VMEM(wu.shape, bf16),
            pltpu.VMEM(wd.shape, bf16),
            pltpu.VMEM((n, slots, width), f32),
            pltpu.VMEM((n, nz, slots, cols), bf16),
            pltpu.VMEM((n, nz, slots, cols), bf16),
            pltpu.VMEM((n, nz, slots, cols), bf16),
            pltpu.VMEM((n, nz, slots, cols), bf16),
            pltpu.VMEM((nz, rows, cols), bf16),
            pltpu.VMEM((nz, rows, cols), bf16),
            dma((3,)),
        ]
        + [dma((n,))] * 8
        + [dma((nz,))] * 2,
        compiler_params=pltpu.CompilerParams(
            collective_id=2, has_side_effects=True, vmem_limit_bytes=48 * 1024 * 1024
        ),
    )(disp, comb, wg, wu, wd)


def per_device(
    resid,
    norm1_gain,
    w_query,
    w_key,
    w_value,
    w_outgate,
    w_igate,
    w_fgate,
    forget_bias,
    head_gain,
    w_out,
    state_matrix,
    state_norm,
    state_max,
    norm2_gain,
    group_router,
    expert_router,
    expert_ids,
    exp_gate,
    exp_up,
    exp_down,
):
    rows = resid.shape[0]
    local_heads = state_matrix.shape[1]
    size = state_matrix.shape[2]
    head_rank = lax.axis_index("tp")
    projected, in_all, forget_all = project(
        resid, norm1_gain, w_query, w_key, w_value, w_outgate, w_igate, w_fgate
    )
    stored = projected.astype(jnp.float32)
    pieces = jnp.split(stored, 4, axis=1)
    scaled = pieces[0].reshape(rows, local_heads, size) * size ** (-0.5)
    key_rows = pieces[1].reshape(rows, local_heads, size)
    value_rows = pieces[2].reshape(rows, local_heads, size)
    outgate = pieces[3].reshape(rows, local_heads, size)
    head_start = head_rank * local_heads
    bias_slice = lax.dynamic_slice_in_dim(forget_bias, head_start, local_heads, 0)
    in_gate = lax.dynamic_slice_in_dim(in_all, head_start, local_heads, 1)
    log_forget = jax.nn.log_sigmoid(
        lax.dynamic_slice_in_dim(forget_all, head_start, local_heads, 1) + bias_slice
    )
    cell_out, new_matrix, new_normer, new_max = memory_cell(
        scaled, key_rows, value_rows, in_gate, log_forget, state_matrix, state_norm, state_max
    )
    headed = cell_out * lax.rsqrt(jnp.mean(cell_out * cell_out, axis=-1, keepdims=True) + EPSILON)
    headed = headed * head_gain.reshape(local_heads, size) * jax.nn.sigmoid(outgate)
    head_out = headed.astype(jnp.bfloat16).reshape(rows, local_heads * size)
    column_count = resid.shape[1] // lax.axis_size("tp")
    own_cols = lax.dynamic_slice_in_dim(resid, head_rank * column_count, column_count, 1)
    after_cols, after_mix = mix(head_out, w_out, own_cols)
    normed2 = rms_scale(after_mix, norm2_gain).astype(jnp.bfloat16)
    experts_all = expert_router.shape[1]
    groups = group_router.shape[1]
    per_group = experts_all // groups
    topk = expert_ids.shape[1]
    group_exp = jnp.exp(jnp.dot(normed2, group_router, preferred_element_type=jnp.float32))
    group_prob = group_exp / jnp.sum(group_exp, axis=1, keepdims=True)
    expert_logits = jnp.dot(normed2, expert_router, preferred_element_type=jnp.float32)
    expert_range = jnp.arange(experts_all, dtype=jnp.int32)
    one_hot = (expert_ids[:, :, None] == expert_range).astype(jnp.float32)
    chosen_exp = jnp.exp(jnp.sum(one_hot * expert_logits[:, None, :], axis=2))
    share = chosen_exp / jnp.sum(chosen_exp, axis=1, keepdims=True)
    group_hot = (
        (expert_ids // per_group)[:, :, None] == jnp.arange(groups, dtype=jnp.int32)
    ).astype(jnp.float32)
    group_weight = jnp.sum(group_hot * group_prob[:, None, :], axis=2)
    route_weight = group_weight * share
    capacity = max(2, 3 * rows * topk // (2 * experts_all))
    capacity = -(-capacity // 16) * 16
    flat_hot = one_hot.reshape(rows * topk, experts_all)
    earlier = jnp.cumsum(flat_hot, axis=0) - flat_hot
    slot = jnp.sum(earlier * flat_hot, axis=1).astype(jnp.int32).reshape(rows, topk)
    position = expert_ids * capacity + slot
    slot_range = jnp.arange(experts_all * capacity, dtype=jnp.int32)
    matched = position[:, :, None] == slot_range
    dispatch = jnp.any(matched, axis=1).astype(jnp.bfloat16)
    ep_count = lax.axis_size("ep")
    spread = matched.astype(jnp.float32) * route_weight[:, :, None]
    combine = jnp.sum(spread, axis=1).reshape(rows, ep_count, -1).transpose(1, 0, 2)
    buffer = jnp.einsum("ts,td->sd", dispatch, normed2, preferred_element_type=jnp.float32).astype(
        jnp.bfloat16
    )
    buffer = buffer.reshape(ep_count, -1, normed2.shape[1])
    moe = experts(buffer, combine, exp_gate, exp_up, exp_down)
    mixed = (after_cols.astype(jnp.float32) + moe).astype(jnp.bfloat16)
    return (mixed, new_matrix, new_normer, new_max)


def solution(mesh):
    in_specs = (
        P("ep", None),
        P(),
        P("ep", "tp"),
        P("ep", "tp"),
        P("ep", "tp"),
        P("ep", "tp"),
        P(),
        P(),
        P(),
        P("tp"),
        P("tp", None),
        P("ep", "tp", None, None),
        P("ep", "tp", None),
        P("ep", "tp"),
        P(),
        P(),
        P(),
        P("ep", None),
        P("ep", None, "tp"),
        P("ep", None, "tp"),
        P("ep", "tp", None),
    )
    out_specs = (P("ep", "tp"), P("ep", "tp", None, None), P("ep", "tp", None), P("ep", "tp"))
    return jax.shard_map(
        per_device, mesh=mesh, in_specs=in_specs, out_specs=out_specs, check_vma=False
    )
```

profile of v0, /device:TPU:0, one launch (start us, length us, event | category | flops | bytes accessed | tf_op | source)
XLA Modules:
  0.0 106.1 jit_solution(7297115318096254786)
XLA Ops:
  0.7 0.8 copy.130
  1.6 0.6 reduce-window.6
  2.2 0.2 slice_reduce_fusion
  2.9 0.7 and_select_fusion
  3.7 1.2 %copy.116.wi = bf16[2048,32]{1,0:T(8,128)(2,1)S(1)} copy(bf16[2048,32]{0,1:T(8,128)(2,1)} %param.27) | data formatting | bytes 262144 | tf_op args[6]
  4.9 1.2 %copy.117.wf = bf16[2048,32]{1,0:T(8,128)(2,1)S(1)} copy(bf16[2048,32]{0,1:T(8,128)(2,1)} %param.28) | data formatting | bytes 262144 | tf_op args[7]
  6.1 1.0 copy-done.5
  7.1 0.9 copy-done.6
  8.1 0.9 copy-done.7
  9.0 0.9 copy-done.8
  10.0 0.9 copy-done.9
  10.9 0.7 copy-done.10
  11.6 24.7 %shard_map.228 = (bf16[128,1024]{1,0:T(8,128)(2,1)S(1)}, f32[128,32]{1,0:T(8,128)S(1)}, f32[128,32]{1,0:T(8,128)S(1)}) custom-call(bf16[128,2048]{1,0:T(8,128)(2,1)S(1)} %copy-done.5, f32[1,2048]{1,0:T(1,128)S(1)} %bitcast.29, bf16[512,256]{1,0:T(8,128)(2,1)S(1)} %copy-done.6, bf16[512,256]{1,0:T(8,128)(2,1)S(1)} %copy-done.7, ...), custom_call_target="tpu_custom_call" | custom-call | tf_op jit(solution)/shard_map/pallas_call | solution.py:109
  36.5 0.8 mul.185
  37.5 0.9 multiply_reduce_fusion.2
  38.5 0.8 copy.119
  39.3 0.7 dynamic_slice.13
  40.2 0.1 abs_maximum_fusion
  40.7 0.7 multiply_add_fusion.1
  41.5 6.8 %multiply_add_fusion = (f32[128,4,64,64]{0,3,2,1:T(8,128)}, f32[128,4,64]{0,2,1:T(8,128)S(1)}) fusion(f32[128,4,64,64]{0,3,2,1:T(8,128)} %param.32, f32[128,4,64]{0,2,1:T(8,128)S(1)} %bitcast.30, f32[128,4,64]{0,2,1:T(8,128)S(1)} %get-tuple-element.37, f32[128,4]{0,1:T(4,128)S(1)} %copy.120, f32[128,4,64]{0,2,1:T(8,128)S(1)} %bitcast.31), kind=kLoop, calls=%fused_computation.1 | loop fusion | flops 10452992 | bytes 17303552 | tf_op jit(solution)/shard_map/add | solution.py:29
  48.5 0.8 constant_dynamic-slice_fusion.own_cols
  49.4 17.7 %shard_map.229 = (bf16[128,256]{1,0:T(8,128)(2,1)S(1)}, bf16[128,2048]{1,0:T(8,128)(2,1)S(1)}) custom-call(bf16[128,256]{1,0:T(8,128)(2,1)S(1)} %copy.129.head, bf16[256,2048]{1,0:T(8,128)(2,1)S(1)} %copy-done.4, bf16[128,256]{1,0:T(8,128)(2,1)S(1)} %constant_dynamic-slice_fusion.own_cols), custom_call_target="tpu_custom_call" | custom-call | tf_op jit(solution)/shard_map/pallas_call | solution.py:203
  67.0 0.2 fusion
  67.3 0.7 convolution_convert_fusion
  67.9 0.3 fusion.17
  68.3 0.3 fusion.12
  68.7 0.1 select_reduce_fusion
  69.1 1.2 %copy-done.2 = bf16[2,2048,128]{2,1,0:T(8,128)(2,1)S(1)} copy-done((bf16[2,2048,128]{2,1,0:T(8,128)(2,1)S(1)}, bf16[2,2048,128]{2,1,0:T(8,128)(2,1)}, u32[]{:S(2)}) %copy-start.2) | copy-done | bytes 1048600
  70.4 1.2 %copy-done.3 = bf16[2,128,2048]{2,1,0:T(8,128)(2,1)S(1)} copy-done((bf16[2,128,2048]{2,1,0:T(8,128)(2,1)S(1)}, bf16[2,128,2048]{2,1,0:T(8,128)(2,1)}, u32[]{:S(2)}) %copy-start.3) | copy-done | bytes 1048600
  71.6 33.2 %shard_map.230 = f32[128,256]{1,0:T(8,128)S(1)} custom-call(bf16[4,96,2048]{2,1,0:T(8,128)(2,1)S(1)} %bitcast.27, f32[4,128,96]{2,1,0:T(8,128)S(1)} %bitcast.28, bf16[2,2048,128]{2,1,0:T(8,128)(2,1)S(1)} %copy-done.1, bf16[2,2048,128]{2,1,0:T(8,128)(2,1)S(1)} %copy-done.2, bf16[2,128,2048]{2,1,0:T(8,128)(2,1)S(1)} %copy-done.3), custom_call_target="tpu_custom_call" | custom-call | tf_op jit(solution)/shard_map/pallas_call | solution.py:343
  104.8 0.6 add_convert_fusion
  105.4 0.7 copy.137
  (57 shorter events, 2.4 us)
Async XLA Ops:
  0.6 67.7 %copy-start = (bf16[2048,8]{0,1:T(8,128)(2,1)S(1)}, bf16[2048,8]{0,1:T(8,128)(2,1)}, u32[]{:S(2)}) copy-start(bf16[2048,8]{0,1:T(8,128)(2,1)} %param.37) | copy-start | bytes 98308
  0.6 40.1 %copy-start.11 = (f32[128,4,64]{0,2,1:T(8,128)S(1)}, f32[128,4,64]{0,2,1:T(8,128)}, u32[]{:S(2)}) copy-start(f32[128,4,64]{0,2,1:T(8,128)} %param.33) | copy-start | bytes 393220
  6.1 1.0 copy-start.5
  7.1 0.9 copy-start.6
  8.1 0.9 copy-start.7
  9.0 0.9 copy-start.8
  10.0 0.9 copy-start.9
  10.9 0.7 copy-start.10
  41.4 7.9 %copy-start.4 = (bf16[256,2048]{1,0:T(8,128)(2,1)S(1)}, bf16[256,2048]{1,0:T(8,128)(2,1)}, u32[]{:S(2)}) copy-start(bf16[256,2048]{1,0:T(8,128)(2,1)} %w.1) | copy-start | bytes 3145732
  41.4 25.8 %copy-start.13 = (f32[2048]{0:T(1024)S(1)}, f32[2048]{0:T(1024)}, u32[]{:S(2)}) copy-start(f32[2048]{0:T(1024)} %param.35) | copy-start | bytes 24580
  41.4 26.5 %copy-start.14 = (bf16[2048,4]{0,1:T(4,128)(2,1)S(1)}, bf16[2048,4]{0,1:T(4,128)(2,1)}, u32[]{:S(2)}) copy-start(bf16[2048,4]{0,1:T(4,128)(2,1)} %param.36) | copy-start | bytes 49156
  41.5 27.2 %copy-start.12 = (s32[128,2]{0,1:T(2,128)S(1)}, s32[128,2]{0,1:T(2,128)}, u32[]{:S(2)}) copy-start(s32[128,2]{0,1:T(2,128)} %param.38) | copy-start | bytes 3076
  41.5 27.7 %copy-start.1 = (bf16[2,2048,128]{2,1,0:T(8,128)(2,1)S(1)}, bf16[2,2048,128]{2,1,0:T(8,128)(2,1)}, u32[]{:S(2)}) copy-start(bf16[2,2048,128]{2,1,0:T(8,128)(2,1)} %wg.1) | copy-start | bytes 3145732
  69.1 1.2 %copy-start.2 = (bf16[2,2048,128]{2,1,0:T(8,128)(2,1)S(1)}, bf16[2,2048,128]{2,1,0:T(8,128)(2,1)}, u32[]{:S(2)}) copy-start(bf16[2,2048,128]{2,1,0:T(8,128)(2,1)} %wu.1) | copy-start | bytes 3145732
  70.4 1.2 %copy-start.3 = (bf16[2,128,2048]{2,1,0:T(8,128)(2,1)S(1)}, bf16[2,128,2048]{2,1,0:T(8,128)(2,1)}, u32[]{:S(2)}) copy-start(bf16[2,128,2048]{2,1,0:T(8,128)(2,1)} %wd.1) | copy-start | bytes 3145732
where the time goes:
time: 107 us; the launch traced here: 106 us
  Pallas kernels  75.5 us (71%)
  local copies, waits for them, and re-layouts  16.9 us (16%)
  other arithmetic  11.4 us (11%)
  matrix products  1.31 us (1%)
    pallas_call x1, Pallas kernels, experts(): pl.pallas_call(functools.partial(expert_kernel, n, nt), out_shape=jax.Sha...  33.2 us
    pallas_call x1, Pallas kernels, project(): pl.pallas_call(functools.partial(project_kernel, n), out_shape=(jax.Shape...  24.7 us
    pallas_call x1, Pallas kernels, mix(): pl.pallas_call(functools.partial(mix_kernel, nt), out_shape=(jax.ShapeDty...  17.7 us
    unnamed x35, local copies, waits for them, and re-layouts  12.6 us
    add x1, other arithmetic, memory_cell(): carried[..., None, None] * matrix  6.78 us

commit v1 on v0

v1 whole, which is shorter than its diff:
```python
import functools

import jax
import jax.numpy as jnp
from jax import lax
from jax.experimental import pallas as pl
from jax.experimental.pallas import tpu as pltpu
from jax.sharding import PartitionSpec as P

EPSILON = 1e-06
MESH = pl.DeviceIdType.MESH
VMEM = pl.BlockSpec(memory_space=pltpu.VMEM)
SMEM = pl.BlockSpec(memory_space=pltpu.SMEM)
HBM = pl.BlockSpec(memory_space=pltpu.HBM)
BF16, F32 = jnp.bfloat16, jnp.float32
DMA = pltpu.SemaphoreType.DMA
ROW = (((1,), (1,)), ((), ()))


def remote(src, dst, send_sem, recv_sem, device):
    return pltpu.make_async_remote_copy(
        src_ref=src,
        dst_ref=dst,
        send_sem=send_sem,
        recv_sem=recv_sem,
        device_id=device,
        device_id_type=MESH,
    )


def in_hbm(*arrays):
    return [pltpu.with_memory_space_constraint(a, pltpu.HBM) for a in arrays]


def in_vmem(*arrays):
    return [pltpu.with_memory_space_constraint(a, pltpu.VMEM) for a in arrays]


def greet(devices):
    barrier = pltpu.get_barrier_semaphore()
    for device in devices:
        pl.semaphore_signal(barrier, inc=1, device_id=device, device_id_type=MESH)


def flip(index, mask):
    out, bit = index, 1
    while bit <= mask:
        if mask & bit:
            out = out + bit - 2 * bit * lax.rem(lax.div(index, bit), 2)
        bit *= 2
    return out


def weight_of(mask):
    return bin(mask).count("1")


def dot(a, b):
    return jnp.dot(a, b, preferred_element_type=F32)


def row_dot(a, b):
    return lax.dot_general(a, b, ROW, preferred_element_type=F32)


def columns(index, width):
    return pl.ds(pl.multiple_of(index * width, width), width)


def halving(n, total):
    bits = max(1, n.bit_length() - 1)
    parts = bits if total % (bits * 128) == 0 else 1
    return [[(p + s) % bits for s in range(bits)] for p in range(parts)]


def project_kernel(
    n, resid_h, gain_h, wq, wk, wv, wo, gi_h, gf_h, bias_h, hgain_h, running_h, normer_h,
    state_h, wout_h,
    out, in_gate, log_forget, hgain, running, normer, state, wout,
    resid, gain, gi, gf, bias, weights, blocks, arrived, acc, snd, rcv, gates,
    wsem, fs, fr, ps, pr, rs, rr,
):
    me, t = lax.axis_index("ep"), lax.axis_index("tp")
    c = lax.rem(t, 2)
    partner = {"tp": t + 1 - 2 * c}
    peers = [{"ep": flip(me, r)} for r in range(n)]
    greet(peers[1:] + [partner])
    depth, width = wq.shape
    heads = in_gate.shape[0]
    plan = [(resid_h, resid), (gain_h, gain)]
    for i, w in enumerate((wq, wk, wv, wo)):
        plan.append((w, weights.at[:, i * width : (i + 1) * width]))
    plan += [
        (gi_h, gi), (gf_h, gf), (hgain_h, hgain), (running_h, running), (normer_h, normer),
        (wout_h, wout), (state_h, state), (bias_h, bias),
    ]
    loads = [pltpu.make_async_copy(src, dst, wsem.at[i]) for i, (src, dst) in enumerate(plan)]
    for load in loads:
        load.start()
    loads[0].wait()
    loads[1].wait()
    wide = resid[...].astype(F32)
    factor = lax.rsqrt(jnp.mean(wide * wide, axis=-1, keepdims=True) + EPSILON)
    normed = (wide * factor * gain[...]).astype(BF16)
    for j in range(n):
        blocks[j] = normed[:, j * depth : (j + 1) * depth]
    half = blocks.shape[1] // 2
    mine = pl.ds(pl.multiple_of(c * half, half), half)
    pl.semaphore_wait(pltpu.get_barrier_semaphore(), n)
    order = sorted(range(1, n), key=lambda r: (-weight_of(r), r))
    forward, pass_on = {}, {}
    for r in order:
        forward[r] = remote(
            blocks.at[flip(me, r), mine, :], arrived.at[r, mine, :], fs.at[r], fr.at[r], peers[r]
        )
        forward[r].start()
    for i in range(2, 8):
        loads[i].wait()
    acc[0] = dot(blocks[me], weights[...])
    loads[13].wait()
    for which, g in enumerate((gi, gf)):
        value = row_dot(g[...], normed)
        for j in range(gates.shape[1]):
            gates[which, j] = value[j * heads : (j + 1) * heads]
    in_gate[...] = gates[0, t]
    for j in range(heads):
        log_forget[j : j + 1, :] = jax.nn.log_sigmoid(
            gates[1, t, j : j + 1, :] + bias[t * heads + j]
        )
    for r in order:
        forward[r].wait_recv()
        pass_on[r] = remote(
            arrived.at[r, mine, :], arrived.at[r, mine, :], ps.at[r], pr.at[r], partner
        )
        pass_on[r].start()
    parts = halving(n, 4 * width)
    wide_part = 4 * width // len(parts)
    back = {}

    def summed(p, r, position):
        value = acc[r, :, p * wide_part : (p + 1) * wide_part]
        for s in range(position):
            bit = 1 << parts[p][s]
            back[p, r | bit].wait_recv()
            value = value + rcv[r | bit, p].astype(F32)
        return value

    def position_of(p, r):
        return min(s for s, b in enumerate(parts[p]) if r >> b & 1)

    sends = [(position_of(p, r), -weight_of(r), r, p) for r in range(1, n) for p in range(len(parts))]
    ready = set()
    for position, _, r, p in sorted(sends):
        if r not in ready:
            pass_on[r].wait_recv()
            acc[r] = dot(arrived[r], weights[...])
            ready.add(r)
        snd[r, p] = summed(p, r, position).astype(BF16)
        back[p, r] = remote(
            snd.at[r, p], rcv.at[r, p], rs.at[p, r], rr.at[p, r], peers[1 << parts[p][position]]
        )
        back[p, r].start()
    for i in range(8, 13):
        loads[i].wait()
    for p in range(len(parts)):
        out[:, p * wide_part : (p + 1) * wide_part] = summed(p, 0, len(parts[p])).astype(BF16)
    for r in order:
        forward[r].wait_send()
        pass_on[r].wait_send()
        for p in range(len(parts)):
            back[p, r].wait_send()


def project(
    resid, gain, wq, wk, wv, wo, gi, gf, bias, hgain, running, normer, state, wout
):
    n, nt = lax.axis_size("ep"), lax.axis_size("tp")
    rows, channels = resid.shape
    depth, width = wq.shape
    heads = state.shape[0]
    parts = len(halving(n, 4 * width))
    vmem = pltpu.VMEM
    return pl.pallas_call(
        functools.partial(project_kernel, n),
        out_shape=(
            vmem((rows, 4 * width), BF16),
            vmem(running.shape, F32),
            vmem(running.shape, F32),
            vmem(hgain.shape, F32),
            vmem(running.shape, F32),
            vmem(normer.shape, F32),
            vmem(state.shape, F32),
            vmem(wout.shape, BF16),
        ),
        in_specs=[HBM] * 14,
        out_specs=(VMEM,) * 8,
        scratch_shapes=[
            vmem((rows, channels), BF16),
            vmem((1, channels), F32),
            vmem(gi.shape, BF16),
            vmem(gf.shape, BF16),
            pltpu.SMEM(bias.shape, F32),
            vmem((depth, 4 * width), BF16),
            vmem((n, rows, depth), BF16),
            vmem((n, rows, depth), BF16),
            vmem((n, rows, 4 * width), F32),
            vmem((n, parts, rows, 4 * width // parts), BF16),
            vmem((n, parts, rows, 4 * width // parts), BF16),
            vmem((2, nt, heads, rows), F32),
            DMA((14,)), DMA((n,)), DMA((n,)), DMA((n,)), DMA((n,)),
            DMA((parts, n)), DMA((parts, n)),
        ],
        compiler_params=pltpu.CompilerParams(
            collective_id=0, has_side_effects=True, vmem_limit_bytes=32 * 1024 * 1024
        ),
    )(
        *in_hbm(
            resid, gain, wq, wk, wv, wo, gi, gf, bias, hgain, running, normer, state, wout
        )
    )


def cell_kernel(
    proj, in_gate, log_forget, state, running, normer, hgain,
    new_matrix_h, new_normer_h, new_max_h, head,
    new_matrix, new_normer, new_max, qs, ks, vs, cell, matrix_sem, small_sem,
):
    heads, size = state.shape[:2]
    width = heads * size
    group = 8
    step = min(128, width)

    def store(h, g):
        part = pl.ds(pl.multiple_of(g * group, group), group)
        return pltpu.make_async_copy(
            new_matrix.at[h, part], new_matrix_h.at[h, part], matrix_sem.at[h, g]
        )

    for i, (dst, scale) in enumerate(((qs, size ** (-0.5)), (ks, None), (vs, None))):
        for j in range(0, width, step):
            value = proj[:, i * width + j : i * width + j + step].astype(F32).T
            dst[j : j + step, :] = value if scale is None else value * scale
    for h in range(heads):
        lines = slice(h * size, (h + 1) * size)
        moved = log_forget[h : h + 1, :] + running[h : h + 1, :]
        stable = jnp.maximum(moved, in_gate[h : h + 1, :])
        fresh = jnp.exp(in_gate[h : h + 1, :] - stable)
        carried = jnp.exp(moved - stable)
        new_max[h : h + 1, :] = stable
        q, k = qs[lines, :], ks[lines, :]
        score = jnp.sum(q * k, axis=0, keepdims=True) * fresh
        denom = carried * jnp.sum(q * normer[h], axis=0, keepdims=True) + score
        k = fresh * k
        ks[lines, :] = k
        new_normer[h] = carried * normer[h] + k

        def some(g, readout, h=h, carried=carried):
            start = pl.multiple_of(g * group, group)
            q8 = qs[pl.ds(h * size + start, group), :]
            k8 = ks[pl.ds(h * size + start, group), :]
            v = vs[h * size : (h + 1) * size, :]
            for i in range(group):
                m = state[h, start + i]
                readout = readout + q8[i : i + 1, :] * m
                new_matrix[h, start + i] = carried * m + k8[i : i + 1, :] * v
            store(h, g).start()
            return readout

        readout = lax.fori_loop(0, size // group, some, jnp.zeros(q.shape, F32))
        value = vs[lines, :]
        out = (carried * readout + score * value) / jnp.maximum(jnp.abs(denom), 1.0)
        factor = lax.rsqrt(jnp.mean(out * out, axis=0, keepdims=True) + EPSILON)
        cell[lines, :] = out * factor
    small = [
        pltpu.make_async_copy(src, dst, small_sem.at[i])
        for i, (src, dst) in enumerate(((new_normer, new_normer_h), (new_max, new_max_h)))
    ]
    for copy in small:
        copy.start()
    for j in range(0, width, step):
        gate = jax.nn.sigmoid(proj[:, 3 * width + j : 3 * width + j + step].astype(F32))
        value = cell[j : j + step, :].T * hgain[:, j : j + step] * gate
        head[:, j : j + step] = value.astype(BF16)
    for copy in small:
        copy.wait()
    for h in range(heads):
        lax.fori_loop(0, size // group, lambda g, x, h=h: (store(h, g).wait(), x)[1], 0)


def memory_cell(proj, in_gate, log_forget, state, running, normer, hgain):
    heads, size, _, rows = state.shape
    width = heads * size
    vmem = pltpu.VMEM
    return pl.pallas_call(
        cell_kernel,
        out_shape=(
            pltpu.HBM(state.shape, F32),
            pltpu.HBM(normer.shape, F32),
            pltpu.HBM(running.shape, F32),
            vmem((rows, width), BF16),
        ),
        in_specs=[VMEM] * 7,
        out_specs=(HBM, HBM, HBM, VMEM),
        scratch_shapes=[
            vmem(state.shape, F32),
            vmem(normer.shape, F32),
            vmem(running.shape, F32),
        ]
        + [vmem((width, rows), F32)] * 4
        + [DMA((heads, size // 8)), DMA((2,))],
        compiler_params=pltpu.CompilerParams(vmem_limit_bytes=24 * 1024 * 1024),
    )(*in_vmem(proj, in_gate, log_forget, state, running, normer, hgain))


def expert_kernel(
    n, nt, cap, groups, per_group,
    head, wout, resid_h, gain_h, group_h, router_h, ids_h, wg, wu, wd,
    out,
    own, gain, grouter, router, ids, wgu, wdown, chosen, chosen_r, scatter,
    pair_s, pair_r, red_s, red_r, gathered, disp, arr, stat, stat_r, msg, msg_r,
    hidden, epair_s, epair_r, ret_s, ret_r, z_s, z_r,
    wsem, hs, hr, ps, pr, rs, rr, gs, gr, ds, dr, fs, fr, ss, sr, ms, mr,
    es, er, bs, br, zs, zr,
):
    me, t = lax.axis_index("ep"), lax.axis_index("tp")
    nz = nt // 2
    z, c = lax.div(t, 2), lax.rem(t, 2)
    partner = {"tp": t + 1 - 2 * c}
    peers = [{"ep": flip(me, r)} for r in range(n)]
    z_at = [flip(z, k) for k in range(nz)]
    z_peers = [{"tp": 2 * z_at[k] + c} for k in range(nz)]
    greet([partner] + peers[1:] + z_peers[1:])
    rows, cols = out.shape
    local, ff = wdown.shape[:2]
    experts = n * local
    fused = len(wgu.shape) == 3
    plan = [
        (resid_h.at[:, columns(t, cols)], own),
        (ids_h, ids),
        (gain_h, gain),
        (group_h, grouter),
        (router_h, router),
    ]
    if fused:
        plan += [(wg, wgu.at[:, :, :ff]), (wu, wgu.at[:, :, ff:])]
    else:
        plan += [(wg, wgu.at[0]), (wu, wgu.at[1])]
    plan.append((wd, wdown))
    loads = [pltpu.make_async_copy(src, dst, wsem.at[i]) for i, (src, dst) in enumerate(plan)]
    for load in loads:
        load.start()

    far = sorted(range(1, nz), reverse=True)
    near = list(range(1, nz))
    away = sorted(range(1, n), key=lambda r: (-weight_of(r), r))

    def mixed_block(dest):
        return dot(head[...], wout[:, columns(dest, cols)])

    for k in far + [0]:
        pair_s[k] = mixed_block(2 * z_at[k] + 1 - c).astype(BF16)
    pl.semaphore_wait(pltpu.get_barrier_semaphore(), 1 + (n - 1) + (nz - 1))
    pair = {}
    for k in far + [0]:
        pair[k] = remote(pair_s.at[k], pair_r.at[k], ps.at[k], pr.at[k], partner)
        pair[k].start()

    loads[1].wait()
    expert_id = lax.broadcasted_iota(jnp.int32, (experts, rows), 0)
    picks = [ids[j : j + 1, :] == expert_id for j in range(ids.shape[0])]
    member = functools.reduce(jnp.logical_or, picks)
    member_f = member.astype(F32)
    before = (
        lax.broadcasted_iota(jnp.int32, (rows, rows), 0)
        < lax.broadcasted_iota(jnp.int32, (rows, rows), 1)
    ).astype(BF16)
    slot = dot(member_f.astype(BF16), before)
    slot = jnp.where(member, slot, -1.0)
    slot_id = lax.broadcasted_iota(jnp.int32, (cap, rows), 0).astype(F32)
    hots = []
    for e in range(experts):
        hots.append((slot[e : e + 1, :] == slot_id).astype(F32))
        chosen[e // local, e % local] = hots[e].astype(BF16)

    reduce = {}
    for k in far + [0]:
        value = mixed_block(2 * z_at[k] + c)
        pair[k].wait_recv()
        value = value + pair_r[k].astype(F32)
        if k > 0:
            red_s[k] = value.astype(BF16)
            reduce[k] = remote(red_s.at[k], red_r.at[k], rs.at[k], rr.at[k], z_peers[k])
            reduce[k].start()
        else:
            total = value
    share = {}
    for r in away:
        share[r] = remote(chosen.at[flip(me, r)], chosen_r.at[r], hs.at[r], hr.at[r], peers[r])
        share[r].start()
    for j in range(n):
        block = jnp.concatenate(hots[j * local : (j + 1) * local], axis=0)
        scatter[j] = block.T.astype(BF16)
    loads[0].wait()
    total = total + own[...].astype(F32)
    for i in range(2, 5):
        loads[i].wait()
    for k in near:
        reduce[k].wait_recv()
        total = total + red_r[k].astype(F32)
    gathered[0] = total.astype(BF16)
    gather = {}
    for k in far:
        gather[k] = remote(gathered.at[0], gathered.at[k], gs.at[k], gr.at[k], z_peers[k])
        gather[k].start()

    send, pass_on = {}, {}
    ones = jnp.ones((8, cols), BF16)

    def dispatch(k):
        if k > 0:
            gather[k].wait_recv()
        at = columns(2 * z_at[k] + c, cols)
        raw = gathered[k].astype(F32)
        scaled = (raw * gain[:, at]).astype(BF16)
        taken = dot(chosen[...].reshape(experts * cap, rows), scaled).astype(BF16)
        disp[k] = taken.reshape(n, local, cap, cols)
        for r in away:
            send[k, r] = remote(
                disp.at[k, flip(me, r)], arr.at[c, k, :, r], ds.at[k, r], dr.at[k, r], peers[r]
            )
            send[k, r].start()
        arr[c, k, :, 0] = disp[k, me]
        forward(k, 0)
        square = raw * raw
        high = square.astype(BF16)
        low = (square - high.astype(F32)).astype(BF16)
        parts = (
            row_dot(ones, high) + row_dot(ones, low),
            row_dot(grouter[:, at], scaled),
            row_dot(router[:, at], scaled),
        )
        for base, part in zip((0, 8, 16), parts):
            lines = slice(base, base + part.shape[0])
            if k == 0:
                stat[lines, :] = part
            else:
                stat[lines, :] += part

    def forward(k, r):
        if r > 0:
            send[k, r].wait_recv()
        pass_on[k, r] = remote(
            arr.at[c, k, :, r], arr.at[c, k, :, r], fs.at[k, r], fr.at[k, r], partner
        )
        pass_on[k, r].start()

    def widen(k, side):
        at = columns(2 * z_at[k] + side, cols)
        for e in range(local):
            x = arr[side, k, e].reshape(n * cap, cols)
            if fused:
                parts = [(slice(0, 2 * ff), dot(x, wgu[e, at, :]))]
            else:
                parts = [
                    (slice(i * ff, (i + 1) * ff), dot(x, wgu[i, e, at, :])) for i in range(2)
                ]
            for lanes, part in parts:
                if k == 0 and first[0]:
                    hidden[e, :, lanes] = part
                else:
                    hidden[e, :, lanes] += part

    first = [True]
    dispatch(0)
    for k in near:
        dispatch(k)
        for r in away:
            forward(k - 1, r)
        if k == 1:
            for i in range(5, 8):
                loads[i].wait()
        widen(k - 1, c)
        first[0] = False
        if k > 1:
            for r in range(n):
                pass_on[k - 2, r].wait_recv()
            widen(k - 2, 1 - c)

    swap = remote(stat, stat_r, ss, sr, partner)
    swap.start()
    swap.wait_recv()

    def summed(base, count):
        lines = slice(base, base + count)
        return stat[lines, :] + stat_r[lines, :]

    factor = lax.rsqrt(summed(0, 1) * (1.0 / (cols * nt)) + EPSILON)
    group_exp = jnp.exp(summed(8, groups) * factor)
    group_prob = group_exp / jnp.sum(group_exp, axis=0, keepdims=True)
    logits = summed(16, experts) * factor
    group_id = lax.broadcasted_iota(jnp.int32, (groups, rows), 0)
    chosen_exp = [
        jnp.exp(jnp.sum(jnp.where(pick, logits, 0.0), axis=0, keepdims=True)) for pick in picks
    ]
    denominator = functools.reduce(jnp.add, chosen_exp)
    expert_weight = jnp.zeros((experts, rows), F32)
    for j, pick in enumerate(picks):
        group_hot = lax.div(ids[j : j + 1, :], per_group) == group_id
        group_share = jnp.sum(jnp.where(group_hot, group_prob, 0.0), axis=0, keepdims=True)
        expert_weight += jnp.where(pick, group_share * (chosen_exp[j] / denominator), 0.0)
    for j in range(n):
        msg[j, 0:1, :] = factor
        msg[j, 1 : 1 + local, :] = expert_weight[j * local : (j + 1) * local, :]
    note = {}
    for r in away:
        note[r] = remote(msg.at[flip(me, r)], msg_r.at[r], ms.at[r], mr.at[r], peers[r])
        note[r].start()
    last = nz - 1
    for r in away:
        forward(last, r)
    widen(last, c)
    if nz > 1:
        for r in range(n):
            pass_on[last - 1, r].wait_recv()
        widen(last - 1, 1 - c)
    columns_of = [[], []]
    weights_of = [[], []]
    columns_of = [[] for _ in range(local)]
    weights_of = [[] for _ in range(local)]
    for r in range(n):
        if r > 0:
            share[r].wait_recv()
            note[r].wait_recv()
        for e in range(local):
            hot = (chosen[me, e] if r == 0 else chosen_r[r, e]).astype(F32)
            words = msg[me] if r == 0 else msg_r[r]
            columns_of[e].append(jnp.sum(hot * words[0:1, :], axis=1, keepdims=True))
            weights_of[e].append(jnp.sum(hot * words[1 + e : 2 + e, :], axis=1, keepdims=True))
    for r in range(n):
        pass_on[last, r].wait_recv()
    widen(last, 1 - c)
    units = []
    for e in range(local):
        scale = jnp.concatenate(columns_of[e], axis=0)
        weight = jnp.concatenate(weights_of[e], axis=0)
        gate = hidden[e, :, :ff] * scale
        up = hidden[e, :, ff:] * scale
        units.append((jax.nn.silu(gate) * up * weight).astype(BF16))

    def down(e, dest):
        return dot(units[e], wdown[e, :, columns(dest, cols)])

    epair, ret, gather_z = {}, {}, {}
    for k in far + [0]:
        for e in range(local):
            epair_s[k, e] = down(e, 2 * z_at[k] + 1 - c).astype(BF16).reshape(n, cap, cols)
        epair[k] = remote(epair_s.at[k], epair_r.at[k], es.at[k], er.at[k], partner)
        epair[k].start()
    for k in far + [0]:
        value = [down(e, 2 * z_at[k] + c).reshape(n, cap, cols) for e in range(local)]
        epair[k].wait_recv()
        for e in range(local):
            ret_s[k, e] = (value[e] + epair_r[k, e].astype(F32)).astype(BF16)
        for r in away:
            ret[k, r] = remote(
                ret_s.at[k, :, r], ret_r.at[k, :, r], bs.at[k, r], br.at[k, r], peers[r]
            )
            ret[k, r].start()
    for k in far + [0]:
        total = gathered[0].astype(F32) if k == 0 else None
        for r in [0] + away[::-1]:
            if r > 0:
                ret[k, r].wait_recv()
            back = ret_s[k, :, 0] if r == 0 else ret_r[k, :, r]
            part = dot(scatter[flip(me, r)], back.reshape(local * cap, cols))
            total = part if total is None else total + part
        if k > 0:
            z_s[k] = total.astype(BF16)
            gather_z[k] = remote(z_s.at[k], z_r.at[k], zs.at[k], zr.at[k], z_peers[k])
            gather_z[k].start()
    for k in far:
        gather_z[k].wait_recv()
        total = total + z_r[k].astype(F32)
    out[...] = total.astype(BF16)

    swap.wait_send()
    for k in range(nz):
        pair[k].wait_send()
        epair[k].wait_send()
        for r in range(n):
            pass_on[k, r].wait_send()
            if r > 0:
                send[k, r].wait_send()
                ret[k, r].wait_send()
        if k > 0:
            reduce[k].wait_send()
            gather[k].wait_send()
            gather_z[k].wait_send()
    for r in away:
        share[r].wait_send()
        note[r].wait_send()


def experts_of(head, wout, resid, gain, group_router, expert_router, ids, wg, wu, wd):
    n, nt = lax.axis_size("ep"), lax.axis_size("tp")
    nz = nt // 2
    rows, channels = resid.shape
    cols = channels // nt
    local, _, ff = wg.shape
    experts = n * local
    groups = group_router.shape[0]
    topk = ids.shape[0]
    cap = max(2, 3 * rows * topk // (2 * experts))
    cap = -(-cap // 16) * 16
    lines = 16 + -(-experts // 8) * 8
    words = 1 + local + -(1 + local) % 8
    wide = (local, channels, 2 * ff) if ff % 128 == 0 else (2, local, channels, ff)
    vmem = pltpu.VMEM
    block = (nz, local, n, cap, cols)
    return pl.pallas_call(
        functools.partial(expert_kernel, n, nt, cap, groups, experts // groups),
        out_shape=jax.ShapeDtypeStruct((rows, cols), BF16),
        in_specs=[VMEM] * 2 + [HBM] * 8,
        out_specs=VMEM,
        scratch_shapes=[
            vmem((rows, cols), BF16),
            vmem((1, channels), F32),
            vmem(group_router.shape, BF16),
            vmem(expert_router.shape, BF16),
            vmem(ids.shape, jnp.int32),
            vmem(wide, BF16),
            vmem(wd.shape, BF16),
            vmem((n, local, cap, rows), BF16),
            vmem((n, local, cap, rows), BF16),
            vmem((n, rows, local * cap), BF16),
            vmem((nz, rows, cols), BF16),
            vmem((nz, rows, cols), BF16),
            vmem((nz, rows, cols), BF16),
            vmem((nz, rows, cols), BF16),
            vmem((nz, rows, cols), BF16),
            vmem((nz, n, local, cap, cols), BF16),
            vmem((2,) + block, BF16),
            vmem((lines, rows), F32),
            vmem((lines, rows), F32),
            vmem((n, words, rows), F32),
            vmem((n, words, rows), F32),
            vmem((local, n * cap, 2 * ff), F32),
            vmem(block, BF16),
            vmem(block, BF16),
            vmem(block, BF16),
            vmem(block, BF16),
            vmem((nz, rows, cols), BF16),
            vmem((nz, rows, cols), BF16),
            DMA((8,)), DMA((n,)), DMA((n,)),
            DMA((nz,)), DMA((nz,)), DMA((nz,)), DMA((nz,)), DMA((nz,)), DMA((nz,)),
            DMA((nz, n)), DMA((nz, n)), DMA((nz, n)), DMA((nz, n)),
            DMA, DMA, DMA((n,)), DMA((n,)),
            DMA((nz,)), DMA((nz,)), DMA((nz, n)), DMA((nz, n)), DMA((nz,)), DMA((nz,)),
        ],
        compiler_params=pltpu.CompilerParams(
            collective_id=1, has_side_effects=True, vmem_limit_bytes=40 * 1024 * 1024
        ),
    )(*in_vmem(head, wout), *in_hbm(resid, gain, group_router, expert_router, ids, wg, wu, wd))


def per_device(
    resid,
    norm1_gain,
    w_query,
    w_key,
    w_value,
    w_outgate,
    w_igate,
    w_fgate,
    forget_bias,
    head_gain,
    w_out,
    state_matrix,
    state_norm,
    state_max,
    norm2_gain,
    group_router,
    expert_router,
    expert_ids,
    exp_gate,
    exp_up,
    exp_down,
):
    proj, in_gate, log_forget, hgain, running, normer, state, wout = project(
        resid, norm1_gain.reshape(1, -1), w_query, w_key, w_value, w_outgate,
        w_igate.T, w_fgate.T, forget_bias, head_gain.reshape(1, -1), state_max.T,
        state_norm.transpose(1, 2, 0), state_matrix.transpose(1, 2, 3, 0), w_out,
    )
    new_matrix, new_normer, new_max, head = memory_cell(
        proj, in_gate, log_forget, state, running, normer, hgain
    )
    mixed = experts_of(
        head, wout, resid, norm2_gain.reshape(1, -1), group_router.T, expert_router.T,
        expert_ids.T, exp_gate, exp_up, exp_down,
    )
    return (
        mixed, new_matrix.transpose(3, 0, 1, 2), new_normer.transpose(2, 0, 1), new_max.T
    )


def solution(mesh):
    in_specs = (
        P("ep", None),
        P(),
        P("ep", "tp"),
        P("ep", "tp"),
        P("ep", "tp"),
        P("ep", "tp"),
        P(),
        P(),
        P(),
        P("tp"),
        P("tp", None),
        P("ep", "tp", None, None),
        P("ep", "tp", None),
        P("ep", "tp"),
        P(),
        P(),
        P(),
        P("ep", None),
        P("ep", None, "tp"),
        P("ep", None, "tp"),
        P("ep", "tp", None),
    )
    out_specs = (P("ep", "tp"), P("ep", "tp", None, None), P("ep", "tp", None), P("ep", "tp"))
    return jax.shard_map(
        per_device, mesh=mesh, in_specs=in_specs, out_specs=out_specs, check_vma=False
    )
```

time: 107 us -> 69.6 us (0.65)
  local copies, waits for them, and re-layouts: 16.9 us -> 0.63 us
  other arithmetic: 11.4 us -> 0 us
  Pallas kernels: 75.5 us -> 68.1 us
  matrix products: 1.31 us -> 0 us
    unnamed x35 -> x1, local copies, waits for them, and re-layouts: 12.6 us -> 0.63 us
    add x2 -> x0, other arithmetic: 7.49 us -> none  [the longest x1 6.78 us: memory_cell(): carried[..., None, None] * matrix]
    pallas_call x3, Pallas kernels: 75.5 us -> 68.1 us  [the longest x1 44.3 us: experts_of(): pl.pallas_call(functools.partial(expert_kernel, n, nt, cap, groups, exper...]
    dynamic_slice x2 -> x0, local copies, waits for them, and re-layouts: 1.58 us -> none  [the longest x1 0.85 us: per_device(): lax.dynamic_slice_in_dim(resid, head_rank * column_count, column_count, 1)]
    reduce_sum x8 -> x0, other arithmetic: 1.49 us -> none  [the longest x1 0.95 us: memory_cell(): denom = carried * jnp.sum(scaled * normer, axis=-1) + score]
    dot_general x3 -> x0, matrix products: 1.31 us -> none  [the longest x1 0.67 us: per_device(): jnp.einsum('ts,td->sd', dispatch, normed2, preferred_element_type=jnp.flo...]
where the time goes in v1:
time: 69.6 us; the launch traced here: 69.4 us
  Pallas kernels  68.1 us (98%)
    pallas_call x1, Pallas kernels, experts_of(): pl.pallas_call(functools.partial(expert_kernel, n, nt, cap, groups, exper...  44.3 us
    pallas_call x1, Pallas kernels, project(): pl.pallas_call(functools.partial(project_kernel, n), out_shape=(vmem((row...  19.9 us
    pallas_call x1, Pallas kernels, memory_cell(): pl.pallas_call(cell_kernel, out_shape=(pltpu.HBM(state.shape, F32), pltpu...  3.87 us

profile of v1, /device:TPU:0, one launch (start us, length us, event | category | flops | bytes accessed | tf_op | source)
XLA Modules:
  0.0 69.4 jit_solution(7242360235685923297)
XLA Ops:
  0.6 19.9 %shard_map.228 = (bf16[128,1024]{1,0:T(8,128)(2,1)S(1)}, f32[4,128]{1,0:T(4,128)S(1)}, f32[4,128]{1,0:T(4,128)S(1)}, f32[1,256]{1,0:T(1,128)S(1)}, f32[4,128]{1,...) custom-call(bf16[128,2048]{1,0:T(8,128)(2,1)} %resid_h.3, ...), custom_call_target="tpu_custom_call" | custom-call | tf_op jit(solution)/shard_map/pallas_call | solution.py:183
  20.6 3.9 %shard_map.229 = (f32[4,64,64,128]{3,2,1,0:T(8,128)}, f32[4,64,128]{2,1,0:T(8,128)}, f32[4,128]{1,0:T(4,128)}, bf16[128,256]{1,0:T(8,128)(2,1)S(1)}) custom-call(bf16[128,1024]{1,0:T(8,128)(2,1)S(1)} %get-tuple-element.16.proj, f32[4,128]{1,0:T(4,128)S(1)} %get-tuple-element.17.in_gate, f32[4,128]{1,0:T(4,128)S(1)} %get-tuple-element.18.log_forget, ...), custom_call_target="tpu_custom_call" | custom-call | tf_op jit(solution)/shard_map/pallas_call | solution.py:294
  24.4 44.3 %shard_map.230 = bf16[128,256]{1,0:T(8,128)(2,1)S(1)} custom-call(bf16[128,256]{1,0:T(8,128)(2,1)S(1)} %get-tuple-element.23.head, bf16[256,2048]{1,0:T(8,128)(2,1)S(1)} %get-tuple-element.24.wout, bf16[128,2048]{1,0:T(8,128)(2,1)} %resid_h.3, f32[1,2048]{1,0:T(1,128)} %bitcast.20, bf16[4,2048]{1,0:T(4,128)(2,1)} %bitcast.19, bf16[8,2048]{1,0:T(8,128)(2,1)} %bitcast.18, ...), custom_call_target="tpu_custom_call" | custom-call | tf_op jit(solution)/shard_map/pallas_call | solution.py:620
  68.8 0.6 copy.26

commit v2 on v1

v2 whole, which is shorter than its diff:
```python
import functools

import jax
import jax.numpy as jnp
from jax import lax
from jax.experimental import pallas as pl
from jax.experimental.pallas import tpu as pltpu
from jax.sharding import PartitionSpec as P

EPSILON = 1e-06
MESH = pl.DeviceIdType.MESH
VMEM = pl.BlockSpec(memory_space=pltpu.VMEM)
SMEM = pl.BlockSpec(memory_space=pltpu.SMEM)
HBM = pl.BlockSpec(memory_space=pltpu.HBM)
BF16, F32 = jnp.bfloat16, jnp.float32
DMA = pltpu.SemaphoreType.DMA
ROW = (((1,), (1,)), ((), ()))


def remote(src, dst, send_sem, recv_sem, device):
    return pltpu.make_async_remote_copy(
        src_ref=src,
        dst_ref=dst,
        send_sem=send_sem,
        recv_sem=recv_sem,
        device_id=device,
        device_id_type=MESH,
    )


def in_hbm(*arrays):
    return [pltpu.with_memory_space_constraint(a, pltpu.HBM) for a in arrays]


def in_vmem(*arrays):
    return [pltpu.with_memory_space_constraint(a, pltpu.VMEM) for a in arrays]


def greet(devices):
    barrier = pltpu.get_barrier_semaphore()
    for device in devices:
        pl.semaphore_signal(barrier, inc=1, device_id=device, device_id_type=MESH)


def flip(index, mask):
    out, bit = index, 1
    while bit <= mask:
        if mask & bit:
            out = out + bit - 2 * bit * lax.rem(lax.div(index, bit), 2)
        bit *= 2
    return out


def weight_of(mask):
    return bin(mask).count("1")


def dot(a, b):
    return jnp.dot(a, b, preferred_element_type=F32)


def row_dot(a, b):
    return lax.dot_general(a, b, ROW, preferred_element_type=F32)


def columns(index, width):
    return pl.ds(pl.multiple_of(index * width, width), width)


def halving(n, total):
    bits = max(1, n.bit_length() - 1)
    parts = bits if total % (bits * 128) == 0 else 1
    return [[(p + s) % bits for s in range(bits)] for p in range(parts)]


def layer_kernel(
    n, nt, cap, groups, per_group,
    resid_h, gain1_h, wq, wk, wv, wo, gi_h, gf_h, bias_h, hgain_h, running_h, normer_h, state_h,
    wout_h, gain2_h, group_h, router_h, ids_h, wg, wu, wd,
    out, new_matrix, new_normer, new_max,
    resid, gain1, gi, gf, bias, hgain, running, normer, state, wout, gain, grouter, router, ids,
    weights, wgu, wdown,
    blocks, arrived, acc, snd, rcv, gates, proj, qs, ks, vs, cell, fades, head,
    own, chosen, chosen_r, scatter,
    pair_s, pair_r, red_s, red_r, gathered, disp, arr, stat, stat_r, msg, msg_r,
    hidden, epair_s, epair_r, ret_s, ret_r, z_s, z_r,
    wsem, as_, ar, qs_, qr, xs, xr,
    hs, hr, ps, pr, rs, rr, gs, gr, ds, dr, fs, fr, ss, sr, ms, mr, es, er, bs, br, zs, zr,
):
    me, t = lax.axis_index("ep"), lax.axis_index("tp")
    nz = nt // 2
    z, c = lax.div(t, 2), lax.rem(t, 2)
    partner = {"tp": t + 1 - 2 * c}
    peers = [{"ep": flip(me, r)} for r in range(n)]
    z_at = [flip(z, k) for k in range(nz)]
    z_peers = [{"tp": 2 * z_at[k] + c} for k in range(nz)]
    greet([partner] + peers[1:] + z_peers[1:])
    rows, cols = out.shape
    local, ff = wdown.shape[:2]
    experts = n * local
    depth, width = wq.shape
    heads, size = state.shape[:2]
    fused = len(wgu.shape) == 3
    batches, lot = snd.shape[0], snd.shape[3]
    lots = [slice(b * lot, (b + 1) * lot) for b in range(batches)]
    far = sorted(range(1, nz), reverse=True)
    near = list(range(1, nz))
    away = sorted(range(1, n), key=lambda r: (-weight_of(r), r))

    plan = {"resid": (resid_h, resid), "gain1": (gain1_h, gain1)}
    for i, w in enumerate((wq, wk, wv, wo)):
        plan[f"w{i}"] = (w, weights.at[:, i * width : (i + 1) * width])
    plan["gi"], plan["gf"], plan["bias"] = (gi_h, gi), (gf_h, gf), (bias_h, bias)
    plan["running"], plan["ids"] = (running_h, running), (ids_h, ids)
    plan["hgain"], plan["normer"] = (hgain_h, hgain), (normer_h, normer)
    plan["state"], plan["wout"] = (state_h, state), (wout_h, wout)
    plan["own"] = (resid_h.at[:, columns(t, cols)], own)
    plan["gain"], plan["group"] = (gain2_h, gain), (group_h, grouter)
    plan["router"] = (router_h, router)
    for i, w in enumerate((wg, wu)):
        plan[f"up{i}"] = (w, wgu.at[:, :, i * ff : (i + 1) * ff] if fused else wgu.at[i])
    plan["down"] = (wd, wdown)
    loads = {
        name: pltpu.make_async_copy(src, dst, wsem.at[i])
        for i, (name, (src, dst)) in enumerate(plan.items())
    }
    for load in loads.values():
        load.start()

    def sent(*kinds):
        for ref, sem in kinds:
            pltpu.make_async_copy(ref, ref, sem).wait()

    def loaded(*names):
        for name in names:
            loads[name].wait()

    loaded("resid", "gain1")
    wide = resid[...].astype(F32)
    factor = lax.rsqrt(jnp.mean(wide * wide, axis=-1, keepdims=True) + EPSILON)
    normed = (wide * factor * gain1[...]).astype(BF16)
    for j in range(n):
        blocks[j] = normed[:, j * depth : (j + 1) * depth]
    half = rows // 2
    mine = pl.ds(pl.multiple_of(c * half, half), half)
    pl.semaphore_wait(pltpu.get_barrier_semaphore(), 1 + (n - 1) + (nz - 1))
    ahead, across = {}, {}
    for r in away:
        ahead[r] = remote(
            blocks.at[flip(me, r), mine, :], arrived.at[r, mine, :], as_, ar.at[r], peers[r]
        )
        ahead[r].start()
    loaded("w0", "w1", "w2", "w3", "gi", "gf", "bias", "running", "ids")
    acc[0] = dot(blocks[me], weights[...])
    for which, g in enumerate((gi, gf)):
        value = row_dot(g[...], normed)
        for j in range(nt):
            gates[which, j] = value[j * heads : (j + 1) * heads]
    for j in range(heads):
        line = slice(j, j + 1)
        in_gate = gates[0, t, line, :]
        forget = jax.nn.log_sigmoid(gates[1, t, line, :] + bias[t * heads + j])
        moved = forget + running[line, :]
        stable = jnp.maximum(moved, in_gate)
        new_max[line, :] = stable
        fades[0, line, :] = jnp.exp(moved - stable)
        fades[1, line, :] = jnp.exp(in_gate - stable)
    proj[...] = jnp.zeros(proj.shape, BF16)
    for r in away:
        ahead[r].wait_recv()
        across[r] = remote(
            arrived.at[r, mine, :], arrived.at[r, mine, :], qs_, qr.at[r], partner
        )
        across[r].start()
    expert_id = lax.broadcasted_iota(jnp.int32, (experts, rows), 0)
    picks = [ids[j : j + 1, :] == expert_id for j in range(ids.shape[0])]
    member = functools.reduce(jnp.logical_or, picks)
    member_f = member.astype(F32)
    before = (
        lax.broadcasted_iota(jnp.int32, (rows, rows), 0)
        < lax.broadcasted_iota(jnp.int32, (rows, rows), 1)
    ).astype(BF16)
    slot = dot(member_f.astype(BF16), before)
    slot = jnp.where(member, slot, -1.0)
    slot_id = lax.broadcasted_iota(jnp.int32, (cap, rows), 0).astype(F32)
    hots = []
    for e in range(experts):
        hots.append((slot[e : e + 1, :] == slot_id).astype(F32))
        chosen[e // local, e % local] = hots[e].astype(BF16)
    for j in range(n):
        block = jnp.concatenate(hots[j * local : (j + 1) * local], axis=0)
        scatter[j] = block.T.astype(BF16)


    parts = halving(n, 4 * width)
    wide_part = 4 * width // len(parts)
    back = {}

    def summed_part(b, p, r, position):
        value = acc[r, lots[b], p * wide_part : (p + 1) * wide_part]
        for s in range(position):
            bit = 1 << parts[p][s]
            back[b, p, r | bit].wait_recv()
            value = value + rcv[b, r | bit, p].astype(F32)
        return value

    steps = {}
    for r in range(1, n):
        for p in range(len(parts)):
            position = min(s for s, bit in enumerate(parts[p]) if r >> bit & 1)
            steps.setdefault((position, -weight_of(r)), []).append((r, p, position))
    order = []
    for i, key in enumerate(sorted(steps)):
        for b in range(batches):
            order.append((max(0, 2 * i - 1) if b == 0 else 2 * i + 2 * b, b, steps[key]))
    ready = {0}
    for _, b, step in sorted(order, key=lambda item: item[:2]):
        for r, p, position in step:
            if r not in ready:
                across[r].wait_recv()
                acc[r] = dot(arrived[r], weights[...])
                ready.add(r)
            snd[b, r, p] = summed_part(b, p, r, position).astype(BF16)
            back[b, p, r] = remote(
                snd.at[b, r, p], rcv.at[b, r, p], xs, xr.at[b, p, r],
                peers[1 << parts[p][position]],
            )
            back[b, p, r].start()

    group = 8
    edge = min(128, heads * size)

    def read(b):
        for p in range(len(parts)):
            value = summed_part(b, p, 0, len(parts[p]))
            proj[lots[b], p * wide_part : (p + 1) * wide_part] = value.astype(BF16)
        for i, dst in enumerate((qs, ks, vs)):
            for j in range(0, width, edge):
                value = proj[:, i * width + j : i * width + j + edge].astype(F32).T
                dst[j : j + edge, :] = value * size ** (-0.5) if i == 0 else value
        for h in range(heads):
            lines = slice(h * size, (h + 1) * size)
            carried, fresh = fades[0, h : h + 1, :], fades[1, h : h + 1, :]
            q = qs[lines, :]
            score = jnp.sum(q * ks[lines, :], axis=0, keepdims=True) * fresh
            denom = carried * jnp.sum(q * normer[h], axis=0, keepdims=True) + score

            def some(g, readout, h=h):
                start = pl.multiple_of(g * group, group)
                q8 = qs[pl.ds(h * size + start, group), :]
                for i in range(group):
                    readout = readout + q8[i : i + 1, :] * state[h, start + i]
                return readout

            readout = lax.fori_loop(0, size // group, some, jnp.zeros(q.shape, F32))
            value = carried * readout + score * vs[lines, :]
            value = value / jnp.maximum(jnp.abs(denom), 1.0)
            mean = jnp.mean(value * value, axis=0, keepdims=True)
            cell[lines, :] = value * lax.rsqrt(mean + EPSILON)
        for j in range(0, width, edge):
            gate = jax.nn.sigmoid(proj[lots[b], 3 * width + j : 3 * width + j + edge].astype(F32))
            value = cell[j : j + edge, :].T[lots[b], :] * hgain[:, j : j + edge] * gate
            head[lots[b], j : j + edge] = value.astype(BF16)

    def renew():
        for h in range(heads):
            lines = slice(h * size, (h + 1) * size)
            carried, fresh = fades[0, h : h + 1, :], fades[1, h : h + 1, :]
            key = fresh * ks[lines, :]
            ks[lines, :] = key
            new_normer[h] = carried * normer[h] + key

            def some(g, x, h=h, carried=carried):
                start = pl.multiple_of(g * group, group)
                k8 = ks[pl.ds(h * size + start, group), :]
                v = vs[h * size : (h + 1) * size, :]
                for i in range(group):
                    new_matrix[h, start + i] = (
                        carried * state[h, start + i] + k8[i : i + 1, :] * v
                    )
                return x

            lax.fori_loop(0, size // group, some, 0)

    pair, reduce, total = {}, {}, {}

    def mixed_block(b, dest):
        return dot(head[lots[b], :], wout[:, columns(dest, cols)])

    def mix(b):
        for k in far + [0]:
            pair_s[b, k] = mixed_block(b, 2 * z_at[k] + 1 - c).astype(BF16)
            pair[b, k] = remote(
                pair_s.at[b, k], pair_r.at[b, k], ps, pr.at[b, k], partner
            )
            pair[b, k].start()
        for k in far + [0]:
            value = mixed_block(b, 2 * z_at[k] + c)
            pair[b, k].wait_recv()
            value = value + pair_r[b, k].astype(F32)
            if k > 0:
                red_s[b, k] = value.astype(BF16)
                reduce[b, k] = remote(
                    red_s.at[b, k], red_r.at[b, k], rs, rr.at[b, k], z_peers[k]
                )
                reduce[b, k].start()
            else:
                total[b] = value + own[lots[b], :].astype(F32)

    loaded("hgain", "normer", "state", "wout", "own")
    for b in range(batches):
        read(b)
        mix(b)
    share = {}
    for r in away:
        share[r] = remote(chosen.at[flip(me, r)], chosen_r.at[r], hs, hr.at[r], peers[r])
        share[r].start()
    renew()
    loaded("gain", "group", "router")
    gather = {}
    for b in range(batches):
        value = total[b]
        for k in near:
            reduce[b, k].wait_recv()
            value = value + red_r[b, k].astype(F32)
        gathered[0, lots[b], :] = value.astype(BF16)
        for k in near:
            gather[b, k] = remote(
                gathered.at[0, lots[b], :], gathered.at[k, lots[b], :],
                gs, gr.at[b, k], z_peers[k],
            )
            gather[b, k].start()

    send, pass_on = {}, {}
    ones = jnp.ones((8, cols), BF16)

    def dispatch(k):
        if k > 0:
            for b in range(batches):
                gather[b, k].wait_recv()
        at = columns(2 * z_at[k] + c, cols)
        raw = gathered[k].astype(F32)
        scaled = (raw * gain[:, at]).astype(BF16)
        taken = dot(chosen[...].reshape(experts * cap, rows), scaled).astype(BF16)
        disp[k] = taken.reshape(n, local, cap, cols)
        for r in away:
            send[k, r] = remote(
                disp.at[k, flip(me, r)], arr.at[c, k, :, r], ds, dr.at[k, r], peers[r]
            )
            send[k, r].start()
        arr[c, k, :, 0] = disp[k, me]
        forward(k, 0)
        square = raw * raw
        high = square.astype(BF16)
        low = (square - high.astype(F32)).astype(BF16)
        parts = (
            row_dot(ones, high) + row_dot(ones, low),
            row_dot(grouter[:, at], scaled),
            row_dot(router[:, at], scaled),
        )
        for base, part in zip((0, 8, 16), parts):
            lines = slice(base, base + part.shape[0])
            if k == 0:
                stat[lines, :] = part
            else:
                stat[lines, :] += part

    def forward(k, r):
        if r > 0:
            send[k, r].wait_recv()
        pass_on[k, r] = remote(
            arr.at[c, k, :, r], arr.at[c, k, :, r], fs, fr.at[k, r], partner
        )
        pass_on[k, r].start()

    def widen(k, side):
        at = columns(2 * z_at[k] + side, cols)
        for e in range(local):
            x = arr[side, k, e].reshape(n * cap, cols)
            if fused:
                parts = [(slice(0, 2 * ff), dot(x, wgu[e, at, :]))]
            else:
                parts = [
                    (slice(i * ff, (i + 1) * ff), dot(x, wgu[i, e, at, :])) for i in range(2)
                ]
            for lanes, part in parts:
                if k == 0 and first[0]:
                    hidden[e, :, lanes] = part
                else:
                    hidden[e, :, lanes] += part

    note, swaps = {}, []

    def announce():
        swap = remote(stat, stat_r, ss, sr, partner)
        swap.start()
        swaps.append(swap)
        swap.wait_recv()

        def summed(base, count):
            lines = slice(base, base + count)
            return stat[lines, :] + stat_r[lines, :]

        factor = lax.rsqrt(summed(0, 1) * (1.0 / (cols * nt)) + EPSILON)
        group_exp = jnp.exp(summed(8, groups) * factor)
        group_prob = group_exp / jnp.sum(group_exp, axis=0, keepdims=True)
        logits = summed(16, experts) * factor
        group_id = lax.broadcasted_iota(jnp.int32, (groups, rows), 0)
        chosen_exp = [
            jnp.exp(jnp.sum(jnp.where(pick, logits, 0.0), axis=0, keepdims=True)) for pick in picks
        ]
        denominator = functools.reduce(jnp.add, chosen_exp)
        expert_weight = jnp.zeros((experts, rows), F32)
        for j, pick in enumerate(picks):
            group_hot = lax.div(ids[j : j + 1, :], per_group) == group_id
            group_share = jnp.sum(jnp.where(group_hot, group_prob, 0.0), axis=0, keepdims=True)
            expert_weight += jnp.where(pick, group_share * (chosen_exp[j] / denominator), 0.0)
        for j in range(n):
            msg[j, 0:1, :] = factor
            msg[j, 1 : 1 + local, :] = expert_weight[j * local : (j + 1) * local, :]
        for r in away:
            note[r] = remote(msg.at[flip(me, r)], msg_r.at[r], ms, mr.at[r], peers[r])
            note[r].start()

    first = [True]
    dispatch(0)
    if nz == 1:
        announce()
    for k in near:
        dispatch(k)
        if k == nz - 1:
            announce()
        for r in away:
            forward(k - 1, r)
        if k == 1:
            loaded("up0", "up1", "down")
        widen(k - 1, c)
        first[0] = False
        if k > 1:
            for r in range(n):
                pass_on[k - 2, r].wait_recv()
            widen(k - 2, 1 - c)

    last = nz - 1
    for r in away:
        forward(last, r)
    widen(last, c)
    if nz > 1:
        for r in range(n):
            pass_on[last - 1, r].wait_recv()
        widen(last - 1, 1 - c)
    columns_of = [[] for _ in range(local)]
    weights_of = [[] for _ in range(local)]
    for r in range(n):
        if r > 0:
            share[r].wait_recv()
            note[r].wait_recv()
        for e in range(local):
            hot = (chosen[me, e] if r == 0 else chosen_r[r, e]).astype(F32)
            words = msg[me] if r == 0 else msg_r[r]
            columns_of[e].append(jnp.sum(hot * words[0:1, :], axis=1, keepdims=True))
            weights_of[e].append(jnp.sum(hot * words[1 + e : 2 + e, :], axis=1, keepdims=True))
    for r in range(n):
        pass_on[last, r].wait_recv()
    widen(last, 1 - c)
    units = []
    for e in range(local):
        scale = jnp.concatenate(columns_of[e], axis=0)
        weight = jnp.concatenate(weights_of[e], axis=0)
        gate = hidden[e, :, :ff] * scale
        up = hidden[e, :, ff:] * scale
        units.append((jax.nn.silu(gate) * up * weight).astype(BF16))

    def down(e, dest):
        return dot(units[e], wdown[e, :, columns(dest, cols)])

    epair, ret, gather_z = {}, {}, {}
    turns = far + [0]

    def offer(k):
        for e in range(local):
            epair_s[k, e] = down(e, 2 * z_at[k] + 1 - c).astype(BF16).reshape(n, cap, cols)
        epair[k] = remote(epair_s.at[k], epair_r.at[k], es, er.at[k], partner)
        epair[k].start()

    offer(turns[0])
    for i, k in enumerate(turns):
        if i + 1 < nz:
            offer(turns[i + 1])
        value = [down(e, 2 * z_at[k] + c).reshape(n, cap, cols) for e in range(local)]
        epair[k].wait_recv()
        for e in range(local):
            ret_s[k, e] = (value[e] + epair_r[k, e].astype(F32)).astype(BF16)
        for r in away:
            ret[k, r] = remote(
                ret_s.at[k, :, r], ret_r.at[k, :, r], bs, br.at[k, r], peers[r]
            )
            ret[k, r].start()
    sent((arrived.at[1:, :half, :], as_), (arrived.at[1:, :half, :], qs_))
    sent((snd.at[:, 1:], xs), (pair_s, ps), (red_s.at[:, 1:], rs), (gathered.at[1:], gs))
    sent((chosen_r.at[1:], hs), (msg_r.at[1:], ms), (disp.at[:, 1:], ds), (arr.at[c], fs))
    sent((stat, ss), (epair_s, es))
    for k in far + [0]:
        total = gathered[0].astype(F32) if k == 0 else None
        for r in [0] + away[::-1]:
            if r > 0:
                ret[k, r].wait_recv()
            back = ret_s[k, :, 0] if r == 0 else ret_r[k, :, r]
            part = dot(scatter[flip(me, r)], back.reshape(local * cap, cols))
            total = part if total is None else total + part
        if k > 0:
            z_s[k] = total.astype(BF16)
            gather_z[k] = remote(z_s.at[k], z_r.at[k], zs, zr.at[k], z_peers[k])
            gather_z[k].start()
    for k in far:
        gather_z[k].wait_recv()
        total = total + z_r[k].astype(F32)
    out[...] = total.astype(BF16)

    sent((ret_s.at[:, :, 1:], bs), (z_s.at[1:], zs))


def layer(
    resid, gain1, wq, wk, wv, wo, gi, gf, bias, hgain, running, normer, state, wout,
    gain2, group_router, expert_router, ids, wg, wu, wd,
):
    n, nt = lax.axis_size("ep"), lax.axis_size("tp")
    nz = nt // 2
    rows, channels = resid.shape
    cols = channels // nt
    depth, width = wq.shape
    heads = state.shape[0]
    local, _, ff = wg.shape
    experts = n * local
    groups = group_router.shape[0]
    topk = ids.shape[0]
    cap = max(2, 3 * rows * topk // (2 * experts))
    cap = -(-cap // 16) * 16
    lines = 16 + -(-experts // 8) * 8
    words = -(-(1 + local) // 8) * 8
    wide = (local, channels, 2 * ff) if ff % 128 == 0 else (2, local, channels, ff)
    parts = len(halving(n, 4 * width))
    batches = 2 if rows % 32 == 0 else 1
    lot = rows // batches
    vmem = pltpu.VMEM
    block = (nz, local, n, cap, cols)
    lot_blocks = (batches, nz, lot, cols)
    returned = (batches, n, parts, lot, 4 * width // parts)
    by_head = (width, rows)
    arrays = (
        resid, gain1, wq, wk, wv, wo, gi, gf, bias, hgain, running, normer, state, wout,
        gain2, group_router, expert_router, ids, wg, wu, wd,
    )
    return pl.pallas_call(
        functools.partial(layer_kernel, n, nt, cap, groups, experts // groups),
        out_shape=(
            vmem((rows, cols), BF16),
            vmem(state.shape, F32),
            vmem(normer.shape, F32),
            vmem(running.shape, F32),
        ),
        in_specs=[HBM] * len(arrays),
        out_specs=(VMEM,) * 4,
        scratch_shapes=[
            vmem((rows, channels), BF16),
            vmem((1, channels), F32),
            vmem(gi.shape, BF16),
            vmem(gf.shape, BF16),
            pltpu.SMEM(bias.shape, F32),
            vmem(hgain.shape, F32),
            vmem(running.shape, F32),
            vmem(normer.shape, F32),
            vmem(state.shape, F32),
            vmem(wout.shape, BF16),
            vmem((1, channels), F32),
            vmem(group_router.shape, BF16),
            vmem(expert_router.shape, BF16),
            vmem(ids.shape, jnp.int32),
            vmem((depth, 4 * width), BF16),
            vmem(wide, BF16),
            vmem(wd.shape, BF16),
            vmem((n, rows, depth), BF16),
            vmem((n, rows, depth), BF16),
            vmem((n, rows, 4 * width), F32),
            vmem(returned, BF16),
            vmem(returned, BF16),
            vmem((2, nt, heads, rows), F32),
            vmem((rows, 4 * width), BF16),
            vmem(by_head, F32),
            vmem(by_head, F32),
            vmem(by_head, F32),
            vmem(by_head, F32),
            vmem((2, heads, rows), F32),
            vmem((rows, width), BF16),
            vmem((rows, cols), BF16),
            vmem((n, local, cap, rows), BF16),
            vmem((n, local, cap, rows), BF16),
            vmem((n, rows, local * cap), BF16),
            vmem(lot_blocks, BF16),
            vmem(lot_blocks, BF16),
            vmem(lot_blocks, BF16),
            vmem(lot_blocks, BF16),
            vmem((nz, rows, cols), BF16),
            vmem((nz, n, local, cap, cols), BF16),
            vmem((2,) + block, BF16),
            vmem((lines, rows), F32),
            vmem((lines, rows), F32),
            vmem((n, words, rows), F32),
            vmem((n, words, rows), F32),
            vmem((local, n * cap, 2 * ff), F32),
            vmem(block, BF16),
            vmem(block, BF16),
            vmem(block, BF16),
            vmem(block, BF16),
            vmem((nz, rows, cols), BF16),
            vmem((nz, rows, cols), BF16),
            DMA((len(arrays) + 1,)),
            DMA, DMA((n,)), DMA, DMA((n,)), DMA, DMA((batches, parts, n)),
            DMA, DMA((n,)), DMA, DMA((batches, nz)), DMA, DMA((batches, nz)),
            DMA, DMA((batches, nz)), DMA, DMA((nz, n)), DMA, DMA((nz, n)),
            DMA, DMA, DMA, DMA((n,)),
            DMA, DMA((nz,)), DMA, DMA((nz, n)), DMA, DMA((nz,)),
        ],
        compiler_params=pltpu.CompilerParams(
            collective_id=0, has_side_effects=True, vmem_limit_bytes=52 * 1024 * 1024
        ),
    )(*in_hbm(*arrays))


def settle_kernel(mixed, matrix, normer, highest, *refs):
    sems = refs[-1]
    pairs = list(zip((mixed, normer, highest), (refs[0], refs[2], refs[3])))
    heads, size = matrix.shape[:2]
    step = size // 4
    for h in range(heads):
        for i in range(0, size, step):
            pairs.append((matrix.at[h, i : i + step], refs[1].at[h, i : i + step]))
    copies = [pltpu.make_async_copy(*pair, sems.at[i]) for i, pair in enumerate(pairs)]
    for copy in copies:
        copy.start()
    for copy in copies:
        copy.wait()


def settle(*arrays):
    return pl.pallas_call(
        settle_kernel,
        out_shape=tuple(pltpu.HBM(a.shape, a.dtype) for a in arrays),
        in_specs=[VMEM] * len(arrays),
        out_specs=(HBM,) * len(arrays),
        scratch_shapes=[DMA((3 + 4 * arrays[1].shape[0],))],
        compiler_params=pltpu.CompilerParams(vmem_limit_bytes=12 * 1024 * 1024),
    )(*in_vmem(*arrays))


def per_device(
    resid,
    norm1_gain,
    w_query,
    w_key,
    w_value,
    w_outgate,
    w_igate,
    w_fgate,
    forget_bias,
    head_gain,
    w_out,
    state_matrix,
    state_norm,
    state_max,
    norm2_gain,
    group_router,
    expert_router,
    expert_ids,
    exp_gate,
    exp_up,
    exp_down,
):
    mixed, new_matrix, new_normer, new_max = settle(
        *layer(
            resid, norm1_gain.reshape(1, -1), w_query, w_key, w_value, w_outgate,
            w_igate.T, w_fgate.T, forget_bias, head_gain.reshape(1, -1), state_max.T,
            state_norm.transpose(1, 2, 0), state_matrix.transpose(1, 2, 3, 0), w_out,
            norm2_gain.reshape(1, -1), group_router.T, expert_router.T, expert_ids.T,
            exp_gate, exp_up, exp_down,
        )
    )
    return (
        mixed, new_matrix.transpose(3, 0, 1, 2), new_normer.transpose(2, 0, 1), new_max.T
    )


def solution(mesh):
    in_specs = (
        P("ep", None),
        P(),
        P("ep", "tp"),
        P("ep", "tp"),
        P("ep", "tp"),
        P("ep", "tp"),
        P(),
        P(),
        P(),
        P("tp"),
        P("tp", None),
        P("ep", "tp", None, None),
        P("ep", "tp", None),
        P("ep", "tp"),
        P(),
        P(),
        P(),
        P("ep", None),
        P("ep", None, "tp"),
        P("ep", None, "tp"),
        P("ep", "tp", None),
    )
    out_specs = (P("ep", "tp"), P("ep", "tp", None, None), P("ep", "tp", None), P("ep", "tp"))
    return jax.shard_map(
        per_device, mesh=mesh, in_specs=in_specs, out_specs=out_specs, check_vma=False
    )
```

time: 69.6 us -> 61.6 us (0.89)
  Pallas kernels: 68.1 us -> 60.8 us
    pallas_call x3 -> x2, Pallas kernels: 68.1 us -> 60.8 us  [the longest x1 57.3 us: layer(): pl.pallas_call(functools.partial(layer_kernel, n, nt, cap, groups, expert...]
where the time goes in v2:
time: 61.6 us; the launch traced here: 61.5 us
  Pallas kernels  60.8 us (99%)
  between operations  0.65 us (1%)
    pallas_call x1, Pallas kernels, layer(): pl.pallas_call(functools.partial(layer_kernel, n, nt, cap, groups, expert...  57.3 us
    pallas_call x1, Pallas kernels, settle(): pl.pallas_call(settle_kernel, out_shape=tuple((pltpu.HBM(a.shape, a.dtype...  3.51 us

profile of v2, /device:TPU:0, one launch (start us, length us, event | category | flops | bytes accessed | tf_op | source)
XLA Modules:
  0.0 61.5 jit_solution(3023406166134448565)
XLA Ops:
  0.6 57.3 %shard_map.228 = (bf16[128,256]{1,0:T(8,128)(2,1)S(1)}, f32[4,64,64,128]{3,2,1,0:T(8,128)S(1)}, f32[4,64,128]{2,1,0:T(8,128)S(1)}, f32[4,128]{1,0:T(4,128)S(1)}) custom-call(bf16[128,2048]{1,0:T(8,128)(2,1)} %resid_h.1, f32[1,2048]{1,0:T(1,128)} %bitcast.20, bf16[512,256]{1,0:T(8,128)(2,1)} %wq.1, bf16[512,256]{1,0:T(8,128)(2,1)} %wk.1, ...), custom_call_target="tpu_custom_call" | custom-call | tf_op jit(solution)/shard_map/pallas_call | solution.py:554
  58.0 3.5 %shard_map.229 = (bf16[128,256]{1,0:T(8,128)(2,1)}, f32[4,64,64,128]{3,2,1,0:T(8,128)}, f32[4,64,128]{2,1,0:T(8,128)}, f32[4,128]{1,0:T(4,128)}) custom-call(bf16[128,256]{1,0:T(8,128)(2,1)S(1)} %get-tuple-element.12.mixed, f32[4,64,64,128]{3,2,1,0:T(8,128)S(1)} %get-tuple-element.13.matrix, f32[4,64,128]{2,1,0:T(8,128)S(1)} %get-tuple-element.14.normer, ...), custom_call_target="tpu_custom_call" | custom-call | tf_op jit(solution)/shard_map/pallas_call | solution.py:646

commit v3 on v2

--- a/solution.py
+++ b/solution.py
@@ -82,10 +82,10 @@
     weights, wgu, wdown,
     blocks, arrived, acc, snd, rcv, gates, proj, qs, ks, vs, cell, fades, head,
     own, chosen, chosen_r, scatter,
-    pair_s, pair_r, red_s, red_r, gathered, disp, arr, stat, stat_r, msg, msg_r,
-    hidden, epair_s, epair_r, ret_s, ret_r, z_s, z_r,
+    wout_far, down_give, head_far, units, red_s, red_r, gathered, disp, arr, stat, stat_r, msg, msg_r,
+    hidden, ret_s, ret_r, z_s, z_r,
     wsem, as_, ar, qs_, qr, xs, xr,
-    hs, hr, ps, pr, rs, rr, gs, gr, ds, dr, fs, fr, ss, sr, ms, mr, es, er, bs, br, zs, zr,
+    hs, hr, ps, pr, ls, lr, rs, rr, gs, gr, ds, dr, fs, fr, ss, sr, ms, mr, es, er, bs, br, zs, zr,
 ):
     me, t = lax.axis_index("ep"), lax.axis_index("tp")
     nz = nt // 2
@@ -96,20 +96,23 @@
     z_peers = [{"tp": 2 * z_at[k] + c} for k in range(nz)]
     greet([partner] + peers[1:] + z_peers[1:])
     rows, cols = out.shape
-    local, ff = wdown.shape[:2]
+    local, ff = down_give.shape[1:3]
     experts = n * local
     depth, width = wq.shape
     heads, size = state.shape[:2]
     fused = len(wgu.shape) == 3
     batches, lot = snd.shape[0], snd.shape[3]
+    sides, band = disp.shape[0], disp.shape[-1]
+    bands = [slice(h * band, (h + 1) * band) for h in range(sides)]
     lots = [slice(b * lot, (b + 1) * lot) for b in range(batches)]
     far = sorted(range(1, nz), reverse=True)
     near = list(range(1, nz))
     away = sorted(range(1, n), key=lambda r: (-weight_of(r), r))
 
-    plan = {"resid": (resid_h, resid), "gain1": (gain1_h, gain1)}
+    plan = {"resid": (resid_h, resid), "norm": (gain1_h, gain1)}
     for i, w in enumerate((wq, wk, wv, wo)):
         plan[f"w{i}"] = (w, weights.at[:, i * width : (i + 1) * width])
+    together = {"w": weights, "up": wgu, "down": down_give, "give": down_give}
     plan["gi"], plan["gf"], plan["bias"] = (gi_h, gi), (gf_h, gf), (bias_h, bias)
     plan["running"], plan["ids"] = (running_h, running), (ids_h, ids)
     plan["hgain"], plan["normer"] = (hgain_h, hgain), (normer_h, normer)
@@ -119,23 +122,27 @@
     plan["router"] = (router_h, router)
     for i, w in enumerate((wg, wu)):
         plan[f"up{i}"] = (w, wgu.at[:, :, i * ff : (i + 1) * ff] if fused else wgu.at[i])
-    plan["down"] = (wd, wdown)
-    loads = {
-        name: pltpu.make_async_copy(src, dst, wsem.at[i])
-        for i, (name, (src, dst)) in enumerate(plan.items())
-    }
-    for load in loads.values():
-        load.start()
+    for k in range(nz):
+        at = columns(2 * z_at[k] + c, cols)
+        plan[f"down{k}"] = (wd.at[:, :, at], wdown.at[k, :, :ff, :])
+        at = columns(2 * z_at[k] + 1 - c, cols)
+        plan[f"give{k}"] = (wd.at[:, :, at], down_give.at[k])
+    loads = {}
+    for name, (src, dst) in plan.items():
+        kind = name.rstrip("0123")
+        known = loads.get(kind)
+        sem = known[1] if known else wsem.at[len(loads)]
+        loads[kind] = (together.get(kind, dst), sem)
+        pltpu.make_async_copy(src, dst, sem).start()
 
     def sent(*kinds):
         for ref, sem in kinds:
             pltpu.make_async_copy(ref, ref, sem).wait()
 
     def loaded(*names):
-        for name in names:
-            loads[name].wait()
-
-    loaded("resid", "gain1")
+        sent(*(loads[name] for name in names))
+
+    loaded("resid", "norm")
     wide = resid[...].astype(F32)
     factor = lax.rsqrt(jnp.mean(wide * wide, axis=-1, keepdims=True) + EPSILON)
     normed = (wide * factor * gain1[...]).astype(BF16)
@@ -147,10 +154,10 @@
     ahead, across = {}, {}
     for r in away:
         ahead[r] = remote(
-            blocks.at[flip(me, r), mine, :], arrived.at[r, mine, :], as_, ar.at[r], peers[r]
+            blocks.at[flip(me, r), mine, :], arrived.at[r, mine, :], as_, ar.at[r - 1], peers[r]
         )
         ahead[r].start()
-    loaded("w0", "w1", "w2", "w3", "gi", "gf", "bias", "running", "ids")
+    loaded("w", "gi", "gf", "bias", "running", "ids")
     acc[0] = dot(blocks[me], weights[...])
     for which, g in enumerate((gi, gf)):
         value = row_dot(g[...], normed)
@@ -169,9 +176,19 @@
     for r in away:
         ahead[r].wait_recv()
         across[r] = remote(
-            arrived.at[r, mine, :], arrived.at[r, mine, :], qs_, qr.at[r], partner
+            arrived.at[r, mine, :], arrived.at[r, mine, :], qs_, qr.at[r - 1], partner
         )
         across[r].start()
+    loaded("wout", "give")
+    lend = []
+    for k in range(nz):
+        at = columns(2 * z_at[k] + 1 - c, cols)
+        lend.append(remote(wout.at[:, at], wout_far.at[k], ls.at[0], lr.at[0], partner))
+        lend.append(
+            remote(down_give.at[k], wdown.at[k, :, ff:, :], ls.at[1], lr.at[1], partner)
+        )
+    for copy in lend:
+        copy.start()
     expert_id = lax.broadcasted_iota(jnp.int32, (experts, rows), 0)
     picks = [ids[j : j + 1, :] == expert_id for j in range(ids.shape[0])]
     member = functools.reduce(jnp.logical_or, picks)
@@ -222,7 +239,7 @@
                 ready.add(r)
             snd[b, r, p] = summed_part(b, p, r, position).astype(BF16)
             back[b, p, r] = remote(
-                snd.at[b, r, p], rcv.at[b, r, p], xs, xr.at[b, p, r],
+                snd.at[b, r, p], rcv.at[b, r, p], xs, xr.at[b, p, r - 1],
                 peers[1 << parts[p][position]],
             )
             back[b, p, r].start()
@@ -284,72 +301,77 @@
 
     pair, reduce, total = {}, {}, {}
 
-    def mixed_block(b, dest):
-        return dot(head[lots[b], :], wout[:, columns(dest, cols)])
-
     def mix(b):
+        pair[b] = remote(
+            head.at[lots[b], :], head_far.at[lots[b], :], ps, pr.at[b], partner
+        )
+        pair[b].start()
+        values = {}
         for k in far + [0]:
-            pair_s[b, k] = mixed_block(b, 2 * z_at[k] + 1 - c).astype(BF16)
-            pair[b, k] = remote(
-                pair_s.at[b, k], pair_r.at[b, k], ps, pr.at[b, k], partner
-            )
-            pair[b, k].start()
+            at = columns(2 * z_at[k] + c, cols)
+            values[k] = dot(head[lots[b], :], wout[:, at])
+        pair[b].wait_recv()
         for k in far + [0]:
-            value = mixed_block(b, 2 * z_at[k] + c)
-            pair[b, k].wait_recv()
-            value = value + pair_r[b, k].astype(F32)
+            value = values[k] + dot(head_far[lots[b], :], wout_far[k])
             if k > 0:
-                red_s[b, k] = value.astype(BF16)
-                reduce[b, k] = remote(
-                    red_s.at[b, k], red_r.at[b, k], rs, rr.at[b, k], z_peers[k]
-                )
-                reduce[b, k].start()
+                for h in range(sides):
+                    red_s[b, k, h] = value[:, bands[h]].astype(BF16)
             else:
                 total[b] = value + own[lots[b], :].astype(F32)
-
-    loaded("hgain", "normer", "state", "wout", "own")
+        for h in range(sides):
+            for k in far:
+                reduce[b, k, h] = remote(
+                    red_s.at[b, k, h], red_r.at[b, k, h], rs, rr.at[b, k - 1, h], z_peers[k]
+                )
+                reduce[b, k, h].start()
+
+    loaded("hgain", "normer", "state", "own")
+    sent((wout_far, lr.at[0]))
     for b in range(batches):
         read(b)
         mix(b)
     share = {}
     for r in away:
-        share[r] = remote(chosen.at[flip(me, r)], chosen_r.at[r], hs, hr.at[r], peers[r])
+        share[r] = remote(chosen.at[flip(me, r)], chosen_r.at[r], hs, hr.at[r - 1], peers[r])
         share[r].start()
     renew()
     loaded("gain", "group", "router")
     gather = {}
-    for b in range(batches):
-        value = total[b]
+
+    def collect(h):
+        for b in range(batches):
+            value = total[b][:, bands[h]]
+            for k in near:
+                reduce[b, k, h].wait_recv()
+                value = value + red_r[b, k, h].astype(F32)
+            gathered[h, 0, lots[b], :] = value.astype(BF16)
         for k in near:
-            reduce[b, k].wait_recv()
-            value = value + red_r[b, k].astype(F32)
-        gathered[0, lots[b], :] = value.astype(BF16)
-        for k in near:
-            gather[b, k] = remote(
-                gathered.at[0, lots[b], :], gathered.at[k, lots[b], :],
-                gs, gr.at[b, k], z_peers[k],
+            gather[h, k] = remote(
+                gathered.at[h, 0], gathered.at[h, k], gs, gr.at[h, k - 1], z_peers[k]
             )
-            gather[b, k].start()
+            gather[h, k].start()
 
     send, pass_on = {}, {}
-    ones = jnp.ones((8, cols), BF16)
-
-    def dispatch(k):
+    ones = jnp.ones((8, band), BF16)
+
+    def lanes_of(h, k, side):
+        start = (2 * z_at[k] + side) * cols + h * band
+        return pl.ds(pl.multiple_of(start, band), band)
+
+    def dispatch(h, k):
         if k > 0:
-            for b in range(batches):
-                gather[b, k].wait_recv()
-        at = columns(2 * z_at[k] + c, cols)
-        raw = gathered[k].astype(F32)
+            gather[h, k].wait_recv()
+        at = lanes_of(h, k, c)
+        raw = gathered[h, k].astype(F32)
         scaled = (raw * gain[:, at]).astype(BF16)
         taken = dot(chosen[...].reshape(experts * cap, rows), scaled).astype(BF16)
-        disp[k] = taken.reshape(n, local, cap, cols)
+        disp[h, k] = taken.reshape(n, local, cap, band)
         for r in away:
-            send[k, r] = remote(
-                disp.at[k, flip(me, r)], arr.at[c, k, :, r], ds, dr.at[k, r], peers[r]
+            send[h, k, r] = remote(
+                disp.at[h, k, flip(me, r)], arr.at[c, h, k, :, r], ds, dr.at[h, k], peers[r]
             )
-            send[k, r].start()
-        arr[c, k, :, 0] = disp[k, me]
-        forward(k, 0)
+            send[h, k, r].start()
+        arr[c, h, k, :, 0] = disp[h, k, me]
         square = raw * raw
         high = square.astype(BF16)
         low = (square - high.astype(F32)).astype(BF16)
@@ -360,23 +382,27 @@
         )
         for base, part in zip((0, 8, 16), parts):
             lines = slice(base, base + part.shape[0])
-            if k == 0:
+            if k + h == 0:
                 stat[lines, :] = part
             else:
                 stat[lines, :] += part
 
-    def forward(k, r):
-        if r > 0:
-            send[k, r].wait_recv()
-        pass_on[k, r] = remote(
-            arr.at[c, k, :, r], arr.at[c, k, :, r], fs, fr.at[k, r], partner
-        )
-        pass_on[k, r].start()
-
-    def widen(k, side):
-        at = columns(2 * z_at[k] + side, cols)
+    def forward(h, k):
+        ref = arr.at[c, h, k, :, 1:]
+        sent((ref, dr.at[h, k]))
+        ref = arr.at[c, h, k]
+        pass_on[h, k] = remote(ref, ref, fs, fr.at[h, k], partner)
+        pass_on[h, k].start()
+        widen(h, k, c)
+
+    def settle_pass(h, k):
+        pass_on[h, k].wait_recv()
+        widen(h, k, 1 - c)
+
+    def widen(h, k, side):
+        at = lanes_of(h, k, side)
         for e in range(local):
-            x = arr[side, k, e].reshape(n * cap, cols)
+            x = arr[side, h, k, e].reshape(n * cap, band)
             if fused:
                 parts = [(slice(0, 2 * ff), dot(x, wgu[e, at, :]))]
             else:
@@ -384,10 +410,11 @@
                     (slice(i * ff, (i + 1) * ff), dot(x, wgu[i, e, at, :])) for i in range(2)
                 ]
             for lanes, part in parts:
-                if k == 0 and first[0]:
+                if first[0]:
                     hidden[e, :, lanes] = part
                 else:
                     hidden[e, :, lanes] += part
+        first[0] = False
 
     note, swaps = {}, []
 
@@ -419,36 +446,22 @@
             msg[j, 0:1, :] = factor
             msg[j, 1 : 1 + local, :] = expert_weight[j * local : (j + 1) * local, :]
         for r in away:
-            note[r] = remote(msg.at[flip(me, r)], msg_r.at[r], ms, mr.at[r], peers[r])
+            note[r] = remote(msg.at[flip(me, r)], msg_r.at[r], ms, mr.at[r - 1], peers[r])
             note[r].start()
 
     first = [True]
-    dispatch(0)
-    if nz == 1:
-        announce()
-    for k in near:
-        dispatch(k)
-        if k == nz - 1:
-            announce()
-        for r in away:
-            forward(k - 1, r)
-        if k == 1:
-            loaded("up0", "up1", "down")
-        widen(k - 1, c)
-        first[0] = False
-        if k > 1:
-            for r in range(n):
-                pass_on[k - 2, r].wait_recv()
-            widen(k - 2, 1 - c)
-
-    last = nz - 1
-    for r in away:
-        forward(last, r)
-    widen(last, c)
-    if nz > 1:
-        for r in range(n):
-            pass_on[last - 1, r].wait_recv()
-        widen(last - 1, 1 - c)
+    items = [(h, 0) for h in range(sides)]
+    items += [(h, k) for h in range(sides) for k in near]
+    for i, (h, k) in enumerate(items):
+        if k == 0:
+            collect(h)
+        dispatch(h, k)
+    announce()
+    loaded("up")
+    for i in range(len(items)):
+        forward(*items[i])
+        if i > 0:
+            settle_pass(*items[i - 1])
     columns_of = [[] for _ in range(local)]
     weights_of = [[] for _ in range(local)]
     for r in range(n):
@@ -460,64 +473,66 @@
             words = msg[me] if r == 0 else msg_r[r]
             columns_of[e].append(jnp.sum(hot * words[0:1, :], axis=1, keepdims=True))
             weights_of[e].append(jnp.sum(hot * words[1 + e : 2 + e, :], axis=1, keepdims=True))
-    for r in range(n):
-        pass_on[last, r].wait_recv()
-    widen(last, 1 - c)
-    units = []
+    settle_pass(*items[-1])
+    share_units = []
     for e in range(local):
         scale = jnp.concatenate(columns_of[e], axis=0)
         weight = jnp.concatenate(weights_of[e], axis=0)
         gate = hidden[e, :, :ff] * scale
         up = hidden[e, :, ff:] * scale
-        units.append((jax.nn.silu(gate) * up * weight).astype(BF16))
-
-    def down(e, dest):
-        return dot(units[e], wdown[e, :, columns(dest, cols)])
-
-    epair, ret, gather_z = {}, {}, {}
-    turns = far + [0]
-
-    def offer(k):
+        units[0, e] = (jax.nn.silu(gate) * up * weight).astype(BF16)
+        copy = remote(units.at[0, e], units.at[1, e], es, er.at[e], partner)
+        copy.start()
+        share_units.append(copy)
+
+    loaded("down")
+    sent((down_give, lr.at[1]))
+    for copy in share_units:
+        copy.wait_recv()
+    ret, gather_z = {}, {}
+    if ff % 128 == 0:
+        both = [jnp.concatenate([units[0, e], units[1, e]], axis=1) for e in range(local)]
+    for k in far + [0]:
         for e in range(local):
-            epair_s[k, e] = down(e, 2 * z_at[k] + 1 - c).astype(BF16).reshape(n, cap, cols)
-        epair[k] = remote(epair_s.at[k], epair_r.at[k], es, er.at[k], partner)
-        epair[k].start()
-
-    offer(turns[0])
-    for i, k in enumerate(turns):
-        if i + 1 < nz:
-            offer(turns[i + 1])
-        value = [down(e, 2 * z_at[k] + c).reshape(n, cap, cols) for e in range(local)]
-        epair[k].wait_recv()
-        for e in range(local):
-            ret_s[k, e] = (value[e] + epair_r[k, e].astype(F32)).astype(BF16)
-        for r in away:
-            ret[k, r] = remote(
-                ret_s.at[k, :, r], ret_r.at[k, :, r], bs, br.at[k, r], peers[r]
-            )
-            ret[k, r].start()
+            if ff % 128 == 0:
+                value = dot(both[e], wdown[k, e])
+            else:
+                value = dot(units[0, e], wdown[k, e, :ff, :]) + dot(
+                    units[1, e], wdown[k, e, ff:, :]
+                )
+            value = value.astype(BF16).reshape(n, cap, cols)
+            for h in range(sides):
+                ret_s[k, h, e] = value[:, :, bands[h]]
+        for h in range(sides):
+            for r in away:
+                ret[k, h, r] = remote(
+                    ret_s.at[k, h, :, r], ret_r.at[k, h, :, r], bs, br.at[k, h], peers[r]
+                )
+                ret[k, h, r].start()
     sent((arrived.at[1:, :half, :], as_), (arrived.at[1:, :half, :], qs_))
-    sent((snd.at[:, 1:], xs), (pair_s, ps), (red_s.at[:, 1:], rs), (gathered.at[1:], gs))
-    sent((chosen_r.at[1:], hs), (msg_r.at[1:], ms), (disp.at[:, 1:], ds), (arr.at[c], fs))
-    sent((stat, ss), (epair_s, es))
+    sent((snd.at[:, 1:], xs), (head, ps), (red_s.at[:, 1:], rs), (gathered.at[:, 1:], gs))
+    sent((chosen_r.at[1:], hs), (msg_r.at[1:], ms), (disp.at[:, :, 1:], ds), (arr.at[c], fs))
+    sent((stat, ss), (units.at[0], es), (wout_far, ls.at[0]), (down_give, ls.at[1]))
     for k in far + [0]:
-        total = gathered[0].astype(F32) if k == 0 else None
-        for r in [0] + away[::-1]:
-            if r > 0:
-                ret[k, r].wait_recv()
-            back = ret_s[k, :, 0] if r == 0 else ret_r[k, :, r]
-            part = dot(scatter[flip(me, r)], back.reshape(local * cap, cols))
-            total = part if total is None else total + part
-        if k > 0:
-            z_s[k] = total.astype(BF16)
-            gather_z[k] = remote(z_s.at[k], z_r.at[k], zs, zr.at[k], z_peers[k])
-            gather_z[k].start()
-    for k in far:
-        gather_z[k].wait_recv()
-        total = total + z_r[k].astype(F32)
-    out[...] = total.astype(BF16)
-
-    sent((ret_s.at[:, :, 1:], bs), (z_s.at[1:], zs))
+        for h in range(sides):
+            total = gathered[h, 0].astype(F32) if k == 0 else None
+            sent((ret_r.at[k, h, :, 1:], br.at[k, h]))
+            for r in range(n):
+                answer = ret_s[k, h, :, 0] if r == 0 else ret_r[k, h, :, r]
+                part = dot(scatter[flip(me, r)], answer.reshape(local * cap, band))
+                total = part if total is None else total + part
+            if k > 0:
+                z_s[k, h] = total.astype(BF16)
+                gather_z[k, h] = remote(
+                    z_s.at[k, h], z_r.at[k, h], zs, zr.at[k - 1, h], z_peers[k]
+                )
+                gather_z[k, h].start()
+            else:
+                for k_from in far:
+                    gather_z[k_from, h].wait_recv()
+                    total = total + z_r[k_from, h].astype(F32)
+                out[:, bands[h]] = total.astype(BF16)
+    sent((ret_s.at[:, :, :, 1:], bs), (z_s.at[1:], zs))
 
 
 def layer(
@@ -543,8 +558,9 @@
     batches = 2 if rows % 32 == 0 else 1
     lot = rows // batches
     vmem = pltpu.VMEM
-    block = (nz, local, n, cap, cols)
-    lot_blocks = (batches, nz, lot, cols)
+    sides = 2 if cols % 256 == 0 else 1
+    band = cols // sides
+    reduced = (batches, nz, sides, lot, band)
     returned = (batches, n, parts, lot, 4 * width // parts)
     by_head = (width, rows)
     arrays = (
@@ -578,7 +594,7 @@
             vmem(ids.shape, jnp.int32),
             vmem((depth, 4 * width), BF16),
             vmem(wide, BF16),
-            vmem(wd.shape, BF16),
+            vmem((nz, local, 2 * ff, cols), BF16),
             vmem((n, rows, depth), BF16),
             vmem((n, rows, depth), BF16),
             vmem((n, rows, 4 * width), F32),
@@ -596,30 +612,31 @@
             vmem((n, local, cap, rows), BF16),
             vmem((n, local, cap, rows), BF16),
             vmem((n, rows, local * cap), BF16),
-            vmem(lot_blocks, BF16),
-            vmem(lot_blocks, BF16),
-            vmem(lot_blocks, BF16),
-            vmem(lot_blocks, BF16),
-            vmem((nz, rows, cols), BF16),
-            vmem((nz, n, local, cap, cols), BF16),
-            vmem((2,) + block, BF16),
+            vmem((nz, width, cols), BF16),
+            vmem((nz, local, ff, cols), BF16),
+            vmem((rows, width), BF16),
+            vmem((2, local, n * cap, ff), BF16),
+            vmem(reduced, BF16),
+            vmem(reduced, BF16),
+            vmem((sides, nz, rows, band), BF16),
+            vmem((sides, nz, n, local, cap, band), BF16),
+            vmem((2, sides, nz, local, n, cap, band), BF16),
             vmem((lines, rows), F32),
             vmem((lines, rows), F32),
             vmem((n, words, rows), F32),
             vmem((n, words, rows), F32),
             vmem((local, n * cap, 2 * ff), F32),
-            vmem(block, BF16),
-            vmem(block, BF16),
-            vmem(block, BF16),
-            vmem(block, BF16),
-            vmem((nz, rows, cols), BF16),
-            vmem((nz, rows, cols), BF16),
-            DMA((len(arrays) + 1,)),
-            DMA, DMA((n,)), DMA, DMA((n,)), DMA, DMA((batches, parts, n)),
-            DMA, DMA((n,)), DMA, DMA((batches, nz)), DMA, DMA((batches, nz)),
-            DMA, DMA((batches, nz)), DMA, DMA((nz, n)), DMA, DMA((nz, n)),
-            DMA, DMA, DMA, DMA((n,)),
-            DMA, DMA((nz,)), DMA, DMA((nz, n)), DMA, DMA((nz,)),
+            vmem((nz, sides, local, n, cap, band), BF16),
+            vmem((nz, sides, local, n, cap, band), BF16),
+            vmem((nz, sides, rows, band), BF16),
+            vmem((nz, sides, rows, band), BF16),
+            DMA((len(arrays),)),
+            DMA, DMA((n - 1,)), DMA, DMA((n - 1,)), DMA, DMA((batches, parts, n - 1)),
+            DMA, DMA((n - 1,)), DMA, DMA((batches,)), DMA((2,)), DMA((2,)),
+            DMA, DMA((batches, nz - 1, sides)),
+            DMA, DMA((sides, nz - 1)), DMA, DMA((sides, nz)), DMA, DMA((sides, nz)),
+            DMA, DMA, DMA, DMA((n - 1,)),
+            DMA, DMA((local,)), DMA, DMA((nz, sides)), DMA, DMA((nz - 1, sides)),
         ],
         compiler_params=pltpu.CompilerParams(
             collective_id=0, has_side_effects=True, vmem_limit_bytes=52 * 1024 * 1024

time: 61.6 us -> 59.7 us (0.969)
  Pallas kernels: 60.8 us -> 59 us
    pallas_call x1, Pallas kernels: 57.3 us -> 55.4 us  [layer(): pl.pallas_call(functools.partial(layer_kernel, n, nt, cap, groups, expert...]
where the time goes in v3:
time: 59.7 us; the launch traced here: 59.6 us
  Pallas kernels  59 us (99%)
  between operations  0.65 us (1%)
    pallas_call x1, Pallas kernels, layer(): pl.pallas_call(functools.partial(layer_kernel, n, nt, cap, groups, expert...  55.4 us
    pallas_call x1, Pallas kernels, settle(): pl.pallas_call(settle_kernel, out_shape=tuple((pltpu.HBM(a.shape, a.dtype...  3.51 us

profile of v3, /device:TPU:0, one launch (start us, length us, event | category | flops | bytes accessed | tf_op | source)
XLA Modules:
  0.0 59.6 jit_solution(17926108965092935171)
XLA Ops:
  0.6 55.4 %shard_map.228 = (bf16[128,256]{1,0:T(8,128)(2,1)S(1)}, f32[4,64,64,128]{3,2,1,0:T(8,128)S(1)}, f32[4,64,128]{2,1,0:T(8,128)S(1)}, f32[4,128]{1,0:T(4,128)S(1)}) custom-call(bf16[128,2048]{1,0:T(8,128)(2,1)} %resid_h.1, f32[1,2048]{1,0:T(1,128)} %bitcast.20, bf16[512,256]{1,0:T(8,128)(2,1)} %wq.1, bf16[512,256]{1,0:T(8,128)(2,1)} %wk.1, ...), custom_call_target="tpu_custom_call" | custom-call | tf_op jit(solution)/shard_map/pallas_call | solution.py:570
  56.1 3.5 %shard_map.229 = (bf16[128,256]{1,0:T(8,128)(2,1)}, f32[4,64,64,128]{3,2,1,0:T(8,128)}, f32[4,64,128]{2,1,0:T(8,128)}, f32[4,128]{1,0:T(4,128)}) custom-call(bf16[128,256]{1,0:T(8,128)(2,1)S(1)} %get-tuple-element.12.mixed, f32[4,64,64,128]{3,2,1,0:T(8,128)S(1)} %get-tuple-element.13.matrix, f32[4,64,128]{2,1,0:T(8,128)S(1)} %get-tuple-element.14.normer, ...), custom_call_target="tpu_custom_call" | custom-call | tf_op jit(solution)/shard_map/pallas_call | solution.py:663
